TPU v7x, 256 devices: a whole 4x4x8 slice. The times are simulated.
256 devices in a mesh: ep: 128 (over z, y, x), tp: 2 (over core).
Axes of the slice: x: 4, y: 4, z: 8, core: 2. Of those that a mesh axis runs over, the one named last changes fastest.
Arguments:
- tokens: bfloat16 [4096, 2048], P('ep'), may hold values from -6 to 6
- lru_state: float32 [4096, 1024], P('ep', 'tp'), may hold values from -6 to 6
- conv_window: bfloat16 [4096, 3, 1024], P('ep', None, 'tp'), may hold values from -6 to 6
- gain_mix_in: float32 [2048], replicated, may hold values from 0.1 to 1.9
- gain_mix_out: float32 [2048], replicated, may hold values from 0.1 to 1.9
- gain_ffn_in: float32 [2048], replicated, may hold values from 0.1 to 1.9
- gain_ffn_out: float32 [2048], replicated, may hold values from 0.1 to 1.9
- w_branch: bfloat16 [2048, 1024], P(None, 'tp'), may hold values from -0.125 to 0.125
- w_input: bfloat16 [2048, 1024], P(None, 'tp'), may hold values from -0.125 to 0.125
- conv_taps: bfloat16 [4, 1024], P(None, 'tp'), may hold values from -3 to 3
- gate_a: bfloat16 [8, 128, 128], P('tp'), may hold values from -0.5 to 0.5
- gate_x: bfloat16 [8, 128, 128], P('tp'), may hold values from -0.5 to 0.5
- decay_rate: float32 [1024], P('tp'), may hold values from 0.001 to 0.3
- w_mix_out: bfloat16 [1024, 2048], P('tp'), may hold values from -0.1875 to 0.1875
- routes: int32 [4096, 4], P('ep'), may hold values from 0 to 127, all different within a row; in each aligned block of 32 rows (0 to 31, 32 to 63, ...) at most 2 rows name the same one
- route_weight: float32 [4096, 4], P('ep'), may hold values from 0.2 to 1.5
- expert_gate: bfloat16 [128, 2048, 512], P('ep', None, 'tp'), may hold values from -0.125 to 0.125
- expert_up: bfloat16 [128, 2048, 512], P('ep', None, 'tp'), may hold values from -0.125 to 0.125
- expert_down: bfloat16 [128, 512, 2048], P('ep', 'tp'), may hold values from -0.25 to 0.25
- shared_gate: bfloat16 [2048, 512], P(None, 'tp'), may hold values from -0.125 to 0.125
- shared_up: bfloat16 [2048, 512], P(None, 'tp'), may hold values from -0.125 to 0.125
- shared_down: bfloat16 [512, 2048], P('tp'), may hold values from -0.25 to 0.25
Outputs:
- layer_out: bfloat16 [4096, 2048], P('ep')
- new_state: float32 [4096, 1024], P('ep', 'tp')
- new_window: bfloat16 [4096, 3, 1024], P('ep', None, 'tp')
Inputs may be any that keep to these rules, and one draw needn't show every extreme that they name: `routes`: each row names 4 different experts. Within the rows of one device (aligned blocks of 32 rows) no expert is named by more than 2 entries, a bound that some block reaches.
All inputs are finite; a program needn't handle non-finite values.
Results may differ from a plain program's by a relative error of at most 0.014.
Values may be sent and summed in bfloat16 or wider, within the bound.
A program may use at most 64 MiB of HBM per device.

v0:
```python
import jax
import jax.numpy as jnp
from jax import lax
from jax.sharding import PartitionSpec as P


def gathered_total(array, axis):
    blocks = lax.all_gather(array, axis).astype(jnp.float32)
    return blocks.sum(axis=0)


def laid_out(blocks, dim):
    shape = list(blocks.shape[1:])
    shape[dim] *= blocks.shape[0]
    return jnp.moveaxis(blocks, 0, dim).reshape(shape)


def copy_for_each(array, axis):
    copies = jnp.broadcast_to(array, (lax.axis_size(axis), *array.shape))
    return lax.all_to_all(copies, axis, split_axis=0, concat_axis=0, tiled=True)


def gather_directly(array, axis, dim):
    return laid_out(copy_for_each(array, axis), dim)


def in_blocks(array, dim, length):
    before, after = (array.shape[:dim], array.shape[dim + 1 :])
    return jnp.moveaxis(array.reshape(*before, length, -1, *after), dim, 0)


def summed_on_arrival(array, axis, dim):
    length = lax.axis_size(axis)
    blocks = lax.all_to_all(in_blocks(array, dim, length), axis, 0, 0, tiled=True)
    return jnp.sum(blocks.astype(jnp.float32), axis=0)


def rms_norm(value, gain):
    return value * lax.rsqrt(jnp.mean(value * value, axis=-1, keepdims=True) + 1e-06) * gain


def rounded_term(value):
    return lax.optimization_barrier(value.astype(jnp.bfloat16)).astype(jnp.float32)


def on_device(
    tokens,
    lru_state,
    conv_window,
    gain_mix_in,
    gain_mix_out,
    gain_ffn_in,
    gain_ffn_out,
    w_branch,
    w_input,
    conv_taps,
    gate_a,
    gate_x,
    decay_rate,
    w_mix_out,
    routes,
    route_weight,
    expert_gate,
    expert_up,
    expert_down,
    shared_gate,
    shared_up,
    shared_down,
):
    resid = tokens.astype(jnp.float32)
    normed = rms_norm(resid, gain_mix_in).astype(jnp.bfloat16)
    branch = jnp.dot(normed, w_branch, preferred_element_type=jnp.float32)
    inflow = jnp.dot(normed, w_input, preferred_element_type=jnp.float32).astype(jnp.bfloat16)
    window = jnp.concatenate([conv_window, inflow[:, None, :]], axis=1)
    new_window = window[:, 1:]
    conv = jnp.sum(window.astype(jnp.float32) * conv_taps.astype(jnp.float32)[None], axis=1)
    count, local_ch = conv.shape
    groups, group_dim = (gate_a.shape[0], gate_a.shape[1])
    grouped = conv.astype(jnp.bfloat16).reshape(count, groups, group_dim)
    recur_gate = jax.nn.sigmoid(
        jnp.einsum("sbi,bij->sbj", grouped, gate_a, preferred_element_type=jnp.float32).reshape(
            count, local_ch
        )
    )
    input_gate = jax.nn.sigmoid(
        jnp.einsum("sbi,bij->sbj", grouped, gate_x, preferred_element_type=jnp.float32).reshape(
            count, local_ch
        )
    )
    log_decay = -8.0 * recur_gate * decay_rate[None]
    new_state = (
        jnp.exp(log_decay) * lru_state + jnp.sqrt(-jnp.expm1(2.0 * log_decay)) * conv * input_gate
    )
    gated = (new_state * jax.nn.gelu(branch)).astype(jnp.bfloat16)
    mix_term = rounded_term(jnp.dot(gated, w_mix_out, preferred_element_type=jnp.float32))
    mixed = gathered_total(mix_term.astype(jnp.bfloat16), "tp").astype(jnp.float32)
    middle = (resid + rms_norm(mixed, gain_mix_out)).astype(jnp.bfloat16)
    ffn_in = rms_norm(middle.astype(jnp.float32), gain_ffn_in).astype(jnp.bfloat16)
    width = ffn_in.shape[1]
    top = routes.shape[1]
    local_exp = expert_gate.shape[0]
    experts = local_exp * lax.axis_size("ep")
    capacity = max(2, 2 * count * top // experts)
    flat = routes.reshape(count * top)
    onehot = (flat[:, None] == jnp.arange(experts, dtype=jnp.int32)[None, :]).astype(jnp.int32)
    rank = jnp.sum(onehot * (jnp.cumsum(onehot, axis=0) - 1), axis=-1)
    dest = flat * capacity + rank
    slot_ids = jnp.arange(experts * capacity, dtype=jnp.int32)
    placed = jnp.any(dest.reshape(count, top)[None, :, :] == slot_ids[:, None, None], axis=-1)
    outbound = jnp.dot(placed.astype(jnp.bfloat16), ffn_in, preferred_element_type=jnp.float32)
    outbound = outbound.astype(jnp.bfloat16).reshape(experts, capacity, width)
    shared_hidden = (
        jax.nn.silu(jnp.dot(ffn_in, shared_gate, preferred_element_type=jnp.float32))
        * jnp.dot(ffn_in, shared_up, preferred_element_type=jnp.float32)
    ).astype(jnp.bfloat16)
    shared = gathered_total(
        rounded_term(
            jnp.dot(shared_hidden, shared_down, preferred_element_type=jnp.float32)
        ).astype(jnp.bfloat16),
        "tp",
    ).astype(jnp.float32)
    share = width // lax.axis_size("tp")
    own = lax.dynamic_slice_in_dim(outbound, lax.axis_index("tp") * share, share, 2)
    arrived = lax.all_to_all(own, "ep", split_axis=0, concat_axis=1, tiled=True)
    rows = gather_directly(arrived, "tp", 2)
    hidden = (
        jax.nn.silu(
            jnp.einsum("erd,edf->erf", rows, expert_gate, preferred_element_type=jnp.float32)
        )
        * jnp.einsum("erd,edf->erf", rows, expert_up, preferred_element_type=jnp.float32)
    ).astype(jnp.bfloat16)
    summed = summed_on_arrival(
        rounded_term(
            jnp.einsum("erf,efd->erd", hidden, expert_down, preferred_element_type=jnp.float32)
        ).astype(jnp.bfloat16),
        "tp",
        2,
    ).astype(jnp.bfloat16)
    back = lax.all_to_all(summed, "ep", split_axis=1, concat_axis=0, tiled=True)
    flat_out = back.reshape(experts * capacity, share)
    picked = flat_out[dest].reshape(count, top, flat_out.shape[1])
    routed_share = jnp.sum(picked.astype(jnp.float32) * route_weight[:, :, None], axis=1).astype(
        jnp.bfloat16
    )
    routed = gather_directly(routed_share, "tp", 1)
    total = routed.astype(jnp.float32) + shared
    layer_out = (middle.astype(jnp.float32) + rms_norm(total, gain_ffn_out)).astype(jnp.bfloat16)
    return (layer_out, new_state, new_window)


def solution(mesh):
    placed = (
        P("ep", None),
        P("ep", "tp"),
        P("ep", None, "tp"),
        P(),
        P(),
        P(),
        P(),
        P(None, "tp"),
        P(None, "tp"),
        P(None, "tp"),
        P("tp", None, None),
        P("tp", None, None),
        P("tp"),
        P("tp", None),
        P("ep", None),
        P("ep", None),
        P("ep", None, "tp"),
        P("ep", None, "tp"),
        P("ep", "tp", None),
        P(None, "tp"),
        P(None, "tp"),
        P("tp", None),
    )
    return jax.shard_map(
        on_device,
        mesh=mesh,
        in_specs=placed,
        out_specs=(P("ep", None), P("ep", "tp"), P("ep", None, "tp")),
        check_vma=False,
    )
```

profile of v0, /device:TPU:1, one launch (start us, length us, event | category | flops | bytes accessed | tf_op | source)
XLA Modules:
  0.0 115.7 jit_solution(3459594786538643539)
XLA Ops:
  0.7 1.2 %fusion.21 = f32[32]{0:T(128)S(1)} fusion(bf16[32,2048]{1,0:T(8,128)(2,1)} %param.22), kind=kLoop, calls=%fused_computation.42 | loop fusion | flops 196576 | bytes 131200 | tf_op jit(solution)/shard_map/reduce_sum | solution.py:39
  2.6 2.2 %fusion.10 = bf16[32,1,512]{2,0,1:T(8,128)(2,1)S(1)} fusion(bf16[2048,512]{1,0:T(8,128)(2,1)} %param.30, bf16[32,2048]{1,0:T(8,128)(2,1)} %param.22, f32[2048]{0:T(1024)} %param.25, f32[32]{0:T(128)S(1)} %add_rsqrt_fusion.3), kind=kOutput, calls=%fused_computation.19 | convolution fusion | flops 67387392 | bytes 2269312 | tf_op jit(solution)/shard_map/dot_general | solution.py:73
  5.4 2.6 %convolution_convert_fusion.3 = bf16[32,2048]{1,0:T(8,128)(2,1)S(1)} fusion(bf16[512,2048]{1,0:T(8,128)(2,1)S(1)} %copy-done, f32[32,512]{1,0:T(8,128)S(1)} %fusion.46, bf16[2048,512]{1,0:T(8,128)(2,1)} %param.29, bf16[32,2048]{1,0:T(8,128)(2,1)S(1)} %copy-done.1, f32[2048]{0:T(1024)S(1)} %copy-done.7, f32[32]{0:T(128)S(1)} %add_rsqrt_fusion.3), kind=kOutput, calls=%fused_computation.5 | convolution fusion | flops 134709248 | bytes 4530304 | tf_op jit(solution)/shard_map/dot_general | solution.py:95
  8.0 4.8 %all-gather = bf16[64,2048]{1,0:T(8,128)(2,1)S(1)} all-gather(bf16[32,2048]{1,0:T(8,128)(2,1)S(1)} %convolution_convert_fusion.3), channel_id=2, replica_groups=mesh['ep'=128,'tp'=2] {'tp'}, dimensions={0}, use_global_device_ids=true | all-gather | bytes 393216 | tf_op jit(solution)/shard_map/all_gather | solution.py:8
  14.7 1.5 %reshape.153 = bf16[128,2,2048]{2,1,0:T(2,128)(2,1)} reshape(bf16[256,2048]{1,0:T(8,128)(2,1)S(1)} %convolution_convert_fusion.1) | data formatting | bytes 2097152 | tf_op jit(solution)/shard_map/reshape | solution.py:111
  16.2 1.4 %constant_dynamic-slice_fusion = bf16[128,2,1024]{2,1,0:T(2,128)(2,1)S(1)} fusion(bf16[128,2,2048]{2,1,0:T(2,128)(2,1)} %reshape.153, s32[]{:T(128)S(6)} %select_n.13), kind=kLoop, calls=%fused_computation.106 | loop fusion | bytes 1048580 | tf_op jit(solution)/shard_map/dynamic_slice | solution.py:123
  17.7 32.4 %all_to_all.36 = bf16[128,2,1024]{2,1,0:T(2,128)(2,1)S(1)} all-to-all(bf16[128,2,1024]{2,1,0:T(2,128)(2,1)S(1)} %constant_dynamic-slice_fusion), channel_id=1, replica_groups=mesh['ep'=128,'tp'=2] {'ep'}, dimensions={0} | all-to-all | bytes 1048576 | tf_op jit(solution)/shard_map/all_to_all | solution.py:124
  50.6 7.1 %all_to_all.37 = bf16[2,1,256,1024]{2,3,1,0:T(8,128)(2,1)S(1)} all-to-all(bf16[2,1,256,1024]{2,3,1,0:T(8,128)(2,1)S(1)} %broadcast_in_dim.7), channel_id=1, replica_groups=mesh['ep'=128,'tp'=2] {'tp'}, dimensions={0} | all-to-all | bytes 2097152 | tf_op jit(solution)/shard_map/all_to_all | solution.py:20
  57.7 1.2 %fusion.14 = f32[256,256]{1,0:T(8,128)} fusion(bf16[256,2048]{0,1:T(8,128)(2,1)S(1)} %bitcast.98, bf16[1,2048,256]{2,1,0:T(8,128)(2,1)S(1)} %copy-done.2), kind=kOutput, calls=%fused_computation.25 | convolution fusion | flops 268435456 | bytes 2359296 | tf_op jit(solution)/shard_map/erd,edf->erf/dot_general | solution.py:128
  58.9 3.9 %fusion = bf16[1,256,2048]{2,1,0:T(8,128)(2,1)} fusion(bf16[1,256,2048]{2,1,0:T(8,128)(2,1)} %param.40, bf16[256,2048]{0,1:T(8,128)(2,1)S(1)} %bitcast.99, bf16[1,2048,256]{2,1,0:T(8,128)(2,1)} %param.39, f32[256,256]{1,0:T(8,128)} %fusion.14), kind=kOutput, calls=%fused_computation.3 | convolution fusion | flops 537788416 | bytes 4456448 | tf_op jit(solution)/shard_map/erf,efd->erd/dot_general | solution.py:134
  62.8 1.3 %copy.110 = bf16[1,32,2,8,1024]{4,3,1,0,2:T(8,128)(2,1)S(1)} copy(bf16[1,32,2,8,1024]{4,3,2,1,0:T(8,128)(2,1)} %bitcast.103) | data formatting | bytes 2097152 | tf_op jit(solution)/shard_map/reshape | solution.py:29
  64.1 4.6 %all_to_all.38 = bf16[2,1,256,1024]{3,2,1,0:T(8,128)(2,1)S(1)} all-to-all(bf16[2,1,256,1024]{3,2,1,0:T(8,128)(2,1)S(1)} %bitcast.100), channel_id=1, replica_groups=mesh['ep'=128,'tp'=2] {'tp'}, dimensions={0} | all-to-all | bytes 2097152 | tf_op jit(solution)/shard_map/all_to_all | solution.py:34
  68.8 1.1 reduce_sum.108
  69.9 1.9 %copy.112 = bf16[1,256,1024]{2,0,1:T(2,128)(2,1)S(1)} copy(bf16[1,256,1024]{2,1,0:T(8,128)(2,1)} %bitcast.102) | data formatting | bytes 1048576 | tf_op jit(solution)/shard_map/reduce_sum | solution.py:35
  72.3 4.5 %reduce.3 = bf16[256,1024]{1,0:T(8,128)(2,1)} reduce(bf16[256,1,1024]{2,1,0:T(2,128)(2,1)S(1)} %bitcast.97, bf16[]{:T(256)} %broadcast.145), dimensions={1}, to_apply=%bitcast.94.reduce_sub_computation | reduce | bytes 1048578
  76.8 2.0 %reshape.174 = bf16[128,2,1024]{2,1,0:T(2,128)(2,1)} reshape(bf16[256,1024]{1,0:T(8,128)(2,1)} %reduce.3) | data formatting | bytes 1048576
  78.8 6.2 %all-to-all-start.3 = ((bf16[128,2,1024]{2,1,0:T(2,128)(2,1)}), bf16[128,2,1024]{2,1,0:T(2,128)(2,1)S(1)}, u32[]{:S(2)}, u32[]{:S(2)}) async-start(bf16[128,2,1024]{2,1,0:T(2,128)(2,1)} %reshape.174), calls=%async_computation.3 | async-start | bytes 1048576 | tf_op jit(solution)/shard_map/all_to_all | solution.py:139
  85.0 1.5 %fusion.79 = f32[32,256]{1,0:T(8,128)S(1)} fusion(bf16[2048,256]{1,0:T(8,128)(2,1)} %param.41, bf16[32,2048]{1,0:T(8,128)(2,1)S(1)} %get-tuple-element.4, f32[2048]{0:T(1024)S(1)} %copy-done.5, f32[32]{0:T(128)S(1)} %add_rsqrt_fusion.1), kind=kOutput, calls=%fused_computation.114 | convolution fusion | flops 33816576 | bytes 1220736 | tf_op jit(solution)/shard_map/dot_general | solution.py:113
  86.8 2.3 %convolution_convert_fusion.2 = bf16[32,2048]{1,0:T(8,128)(2,1)S(1)} fusion(bf16[256,2048]{1,0:T(8,128)(2,1)} %param.43, bf16[2048,256]{1,0:T(8,128)(2,1)} %param.42, f32[32,256]{1,0:T(8,128)S(1)} %fusion.79, bf16[32,2048]{1,0:T(8,128)(2,1)S(1)} %get-tuple-element.4, f32[2048]{0:T(1024)S(1)} %copy-done.5, f32[32]{0:T(128)S(1)} %add_rsqrt_fusion.1), kind=kOutput, calls=%fused_computation.4 | convolution fusion | flops 67485696 | bytes 2400384 | tf_op jit(solution)/shard_map/dot_general | solution.py:118
  89.1 2.0 %all-gather.1 = bf16[64,2048]{1,0:T(8,128)(2,1)S(1)} all-gather(bf16[32,2048]{1,0:T(8,128)(2,1)S(1)} %convolution_convert_fusion.2), channel_id=3, replica_groups=mesh['ep'=128,'tp'=2] {'tp'}, dimensions={0}, use_global_device_ids=true | all-gather | bytes 393216 | tf_op jit(solution)/shard_map/all_gather | solution.py:8
  91.8 12.5 %all-to-all-done.3 = bf16[128,2,1024]{2,1,0:T(2,128)(2,1)S(1)} async-done(((bf16[128,2,1024]{2,1,0:T(2,128)(2,1)}), bf16[128,2,1024]{2,1,0:T(2,128)(2,1)S(1)}, u32[]{:S(2)}, u32[]{:S(2)}) %all-to-all-start.3) | async-done | bytes 524320 | tf_op jit(solution)/shard_map/all_to_all | solution.py:139
  104.2 1.7 %reshape.175 = bf16[256,1,1024]{2,1,0:T(2,128)(2,1)} reshape(bf16[128,2,1024]{2,1,0:T(2,128)(2,1)S(1)} %all-to-all-done.3) | data formatting | bytes 1048576
  105.9 1.4 %copy.111 = bf16[1,256,1024]{2,1,0:T(8,128)(2,1)S(1)} copy(bf16[1,256,1024]{2,0,1:T(2,128)(2,1)} %bitcast.96) | data formatting | bytes 1048576
  108.8 5.9 %all_to_all.39 = bf16[2,32,1024]{2,1,0:T(8,128)(2,1)S(1)} all-to-all(bf16[2,32,1024]{2,1,0:T(8,128)(2,1)S(1)} %broadcast_in_dim.8), channel_id=1, replica_groups=mesh['ep'=128,'tp'=2] {'tp'}, dimensions={0} | all-to-all | bytes 262144 | tf_op jit(solution)/shard_map/all_to_all | solution.py:20
  (71 shorter events, 7.3 us)
Async XLA Ops:
  0.6 4.7 %copy-start = (bf16[512,2048]{1,0:T(8,128)(2,1)S(1)}, bf16[512,2048]{1,0:T(8,128)(2,1)}, u32[]{:S(2)}) copy-start(bf16[512,2048]{1,0:T(8,128)(2,1)} %param.35) | copy-start | bytes 6291460
  0.6 4.7 %copy-start.1 = (bf16[32,2048]{1,0:T(8,128)(2,1)S(1)}, bf16[32,2048]{1,0:T(8,128)(2,1)}, u32[]{:S(2)}) copy-start(bf16[32,2048]{1,0:T(8,128)(2,1)} %param.22) | copy-start | bytes 393220
  0.7 4.7 %copy-start.7 = (f32[2048]{0:T(1024)S(1)}, f32[2048]{0:T(1024)}, u32[]{:S(2)}) copy-start(f32[2048]{0:T(1024)} %param.25) | copy-start | bytes 24580
  0.7 4.2 %copy-start.3 = (bf16[32,3,512]{2,0,1:T(8,128)(2,1)S(1)}, bf16[32,3,512]{2,0,1:T(8,128)(2,1)}, u32[]{:S(2)}) copy-start(bf16[32,3,512]{2,0,1:T(8,128)(2,1)} %param.24) | copy-start | bytes 294916
  0.7 4.2 %copy-start.13 = (bf16[4,128,128]{2,1,0:T(8,128)(2,1)S(1)}, bf16[4,128,128]{2,1,0:T(8,128)(2,1)}, u32[]{:S(2)}) copy-start(bf16[4,128,128]{2,1,0:T(8,128)(2,1)} %param.33) | copy-start | bytes 393220
  0.7 4.4 %copy-start.14 = (bf16[4,128,128]{2,1,0:T(8,128)(2,1)S(1)}, bf16[4,128,128]{2,1,0:T(8,128)(2,1)}, u32[]{:S(2)}) copy-start(bf16[4,128,128]{2,1,0:T(8,128)(2,1)} %param.32) | copy-start | bytes 393220
  0.7 4.5 %copy-start.12 = (f32[512]{0:T(512)S(1)}, f32[512]{0:T(512)}, u32[]{:S(2)}) copy-start(f32[512]{0:T(512)} %param.34) | copy-start | bytes 6148
  0.7 4.5 %copy-start.6 = (f32[32,512]{1,0:T(8,128)S(1)}, f32[32,512]{1,0:T(8,128)}, u32[]{:S(2)}) copy-start(f32[32,512]{1,0:T(8,128)} %param.23) | copy-start | bytes 196612
  5.4 2.6 %copy-start.4 = (f32[32,512]{1,0:T(8,128)}, f32[32,512]{1,0:T(8,128)S(1)}, u32[]{:S(2)}) copy-start(f32[32,512]{1,0:T(8,128)S(1)} %fusion.46) | copy-start | bytes 196612
  5.4 7.6 %copy-start.8 = (f32[2048]{0:T(1024)S(1)}, f32[2048]{0:T(1024)}, u32[]{:S(2)}) copy-start(f32[2048]{0:T(1024)} %param.26) | copy-start | bytes 24580
  5.4 7.9 %copy-start.10 = (s32[32,4]{0,1:T(4,128)S(1)}, s32[32,4]{0,1:T(4,128)}, u32[]{:S(2)}) copy-start(s32[32,4]{0,1:T(4,128)} %param.36) | copy-start | bytes 1540
  8.0 6.2 %copy-start.5 = (f32[2048]{0:T(1024)S(1)}, f32[2048]{0:T(1024)}, u32[]{:S(2)}) copy-start(f32[2048]{0:T(1024)} %param.27) | copy-start | bytes 24580
  50.5 7.2 %copy-start.2 = (bf16[1,2048,256]{2,1,0:T(8,128)(2,1)S(1)}, bf16[1,2048,256]{2,1,0:T(8,128)(2,1)}, u32[]{:S(2)}) copy-start(bf16[1,2048,256]{2,1,0:T(8,128)(2,1)} %param.38) | copy-start | bytes 3145732
  72.3 14.4 %copy-start.11 = (f32[32,4]{0,1:T(4,128)S(1)}, f32[32,4]{0,1:T(4,128)}, u32[]{:S(2)}) copy-start(f32[32,4]{0,1:T(4,128)} %param.37) | copy-start | bytes 1540
  78.8 25.4 %all-to-all-start.3 = ((bf16[128,2,1024]{2,1,0:T(2,128)(2,1)}), bf16[128,2,1024]{2,1,0:T(2,128)(2,1)S(1)}, u32[]{:S(2)}, u32[]{:S(2)}) async-start(bf16[128,2,1024]{2,1,0:T(2,128)(2,1)} %reshape.174), calls=%async_computation.3 | async-start | bytes 1048576 | tf_op jit(solution)/shard_map/all_to_all | solution.py:139
  108.2 6.7 %copy-start.9 = (f32[2048]{0:T(1024)S(1)}, f32[2048]{0:T(1024)}, u32[]{:S(2)}) copy-start(f32[2048]{0:T(1024)} %param.28) | copy-start | bytes 24580
where the time goes:
time: 117 us; the launch traced here: 116 us
  blocking collectives  56.9 us (49%)
  matrix products  14.6 us (12%)
  local copies, waits for them, and re-layouts  13.9 us (12%)
  waiting for transfers between devices  12.5 us (11%)
  other arithmetic  10.6 us (9%)
  starting transfers between devices  6.17 us (5%)
    all_to_all x1, blocking collectives, on_device(): arrived = lax.all_to_all(own, 'ep', split_axis=0, concat_axis=1, tiled=True)  32.4 us
    all_to_all x2, blocking collectives, copy_for_each(): return lax.all_to_all(copies, axis, split_axis=0, concat_axis=0, tiled=True)  13 us
    all_to_all x1, waiting for transfers between devices, on_device(): back = lax.all_to_all(summed, 'ep', split_axis=1, concat_axis=0, tiled=True)  12.5 us
    all_gather x2, blocking collectives, gathered_total(): blocks = lax.all_gather(array, axis).astype(jnp.float32)  6.83 us
    all_to_all x1, starting transfers between devices, on_device(): back = lax.all_to_all(summed, 'ep', split_axis=1, concat_axis=0, tiled=True)  6.17 us
    unnamed x36, local copies, waits for them, and re-layouts  5.94 us
    all_to_all x1, blocking collectives, summed_on_arrival(): lax.all_to_all(in_blocks(array, dim, length), axis, 0, 0, tiled=True)  4.63 us
    unnamed x2, other arithmetic  4.52 us
  transfers between devices with their start and end apart: 1, of which 1 were waited for; matrix products, arithmetic and copies ran while one was open for 4% of the time, Pallas kernels for 0%

commit v1 on v0

v1 whole, which is shorter than its diff:
```python
import functools

import jax
import jax.numpy as jnp
from jax import lax
from jax.experimental import pallas as pl
from jax.experimental.pallas import tpu as pltpu
from jax.sharding import PartitionSpec as P

MESH = pl.DeviceIdType.MESH
F32 = jnp.float32
BF16 = jnp.bfloat16

NZ = 8
NQ = 16
SEQ = 32
TOP = 4
D = 2048
HALF = D // 2
NCH = 2
CW = HALF // NCH
LC = 512
HID = 256
ROWS = NZ * 2
NPIECE = 4


def scaled(value, gain):
    return value * lax.rsqrt(jnp.mean(value * value, axis=-1, keepdims=True) + 1e-06) * gain


def dot(a, b):
    return jnp.dot(a, b, preferred_element_type=F32)


def kernel(
    tok_h, lru_h, convp_h, taps_h, gains_h, decay_h, wb_h, wi_h, ga_h, gx_h, wm_h, routes_h, meta_h,
    eg_h, eu_h, ed_h, sg_h, su_h, sd_h,
    out_h, state_h, inflow_h,
    tok, lru, convp, taps, gains, decay, wb, wi, ga, gx, wm, routes, meta_in,
    eg, eu, ed, sg, su, sd,
    state_v, inflow_v, out_v, middle_v, ffn,
    mix_s, mix_r, meta_s, meta_r, sh_s, sh_r,
    g_buf, r_buf, x_buf, p_buf, whi, wlo, hid_v, y_s, y_r, o_buf, b_buf, t_buf, v_buf, rt_buf,
    lsem, osem,
    tp_s, tp_r, ms_s, ms_r, za_s, za_r, xa_s, xa_r, xf_s, xf_r, yx_s, yx_r, xb_s, xb_r, zb_s, zb_r, rt_s, rt_r,
):
    me = lax.axis_index("ep")
    c = lax.axis_index("tp")
    z = me // NQ
    q = me % NQ
    y, x = q // 4, q % 4

    def z_peer(i):
        return lax.rem(z + i, NZ)

    def q_peer(i):
        return lax.rem(y + i // 4, 4) * 4 + lax.rem(x + i % 4, 4)

    def rows(i, n):
        return pl.ds(pl.multiple_of(i * n, n), n)

    barrier = pltpu.get_barrier_semaphore()
    pl.semaphore_signal(barrier, inc=1, device_id=(me, 1 - c), device_id_type=MESH)

    def greet_z(i, carry):
        pl.semaphore_signal(barrier, inc=1, device_id=(z_peer(i) * NQ + q, c), device_id_type=MESH)
        return carry

    def greet_q(i, carry):
        pl.semaphore_signal(barrier, inc=1, device_id=(z * NQ + q_peer(i), c), device_id_type=MESH)
        return carry

    lax.fori_loop(1, NZ, greet_z, 0)
    lax.fori_loop(1, NQ, greet_q, 0)

    def load(k, src, dst):
        copy = pltpu.make_async_copy(src, dst, lsem.at[k])
        copy.start()
        return copy

    step = D // NPIECE
    l_tok = load(0, tok_h, tok)
    l_gains = load(1, gains_h, gains)
    l_wi = [load(2 + i, wi_h.at[pl.ds(i * step, step)], wi.at[pl.ds(i * step, step)]) for i in range(NPIECE)]
    l_convp = load(6, convp_h, convp)
    l_taps = load(7, taps_h, taps)
    l_ga = load(8, ga_h, ga)
    l_gx = load(9, gx_h, gx)
    l_wb = [load(10 + i, wb_h.at[pl.ds(i * step, step)], wb.at[pl.ds(i * step, step)]) for i in range(NPIECE)]
    l_decay = load(14, decay_h, decay)
    l_lru = load(15, lru_h, lru)
    l_routes = load(16, routes_h, routes)
    l_meta = load(17, meta_h, meta_in)
    l_wm = load(18, wm_h, wm)

    l_routes.wait()
    l_meta.wait()
    lane = lax.broadcasted_iota(jnp.int32, (1, NZ * SEQ), 1)
    mine = (lane // SEQ) == z
    earlier = lax.broadcasted_iota(jnp.int32, (SEQ, NZ * SEQ), 0) < (lane % SEQ)
    named = routes[...].astype(F32)
    for k in range(TOP):
        expert = meta_in[k : k + 1, :]
        same = named[:, 0:1] == expert
        for j in range(1, TOP):
            same = same | (named[:, j : j + 1] == expert)
        rank = jnp.sum(jnp.where(same & earlier, 1.0, 0.0), axis=0, keepdims=True)
        meta_s[k : k + 1, :] = jnp.where(mine, 2.0 * expert + rank, 0.0)
    meta_s[TOP : 2 * TOP, :] = jnp.where(mine, meta_in[TOP : 2 * TOP, :], 0.0)
    meta_r[pl.ds(z, 1)] = meta_s[...][None]

    l_tok.wait()
    l_gains.wait()
    normed = scaled(tok[...].astype(F32), gains[0:1, :]).astype(BF16)
    inflow = jnp.zeros((SEQ, LC), F32)
    for i in range(NPIECE):
        l_wi[i].wait()
        inflow += dot(normed[:, i * step : (i + 1) * step], wi[i * step : (i + 1) * step, :])
    inflow = inflow.astype(BF16)
    inflow_v[...] = inflow
    o_inflow = pltpu.make_async_copy(inflow_v, inflow_h, osem.at[0])
    o_inflow.start()
    l_convp.wait()
    l_taps.wait()
    conv = convp[...] + inflow.astype(F32) * taps[3:4, :].astype(F32)
    low = conv.astype(BF16)
    l_ga.wait()
    l_gx.wait()
    groups = LC // 128
    recur = [dot(low[:, g * 128 : (g + 1) * 128], ga[g]) for g in range(groups)]
    inputs = [dot(low[:, g * 128 : (g + 1) * 128], gx[g]) for g in range(groups)]
    recur_gate = jax.nn.sigmoid(jnp.concatenate(recur, axis=1))
    input_gate = jax.nn.sigmoid(jnp.concatenate(inputs, axis=1))
    l_decay.wait()
    l_lru.wait()
    fall = 8.0 * recur_gate * decay[...]
    t = jnp.tanh(fall)
    state = jnp.exp(-fall) * lru[...] + jnp.sqrt(2.0 * t / (1.0 + t)) * conv * input_gate
    state_v[...] = state
    o_state = pltpu.make_async_copy(state_v, state_h, osem.at[1])
    o_state.start()
    branch = jnp.zeros((SEQ, LC), F32)
    for i in range(NPIECE):
        l_wb[i].wait()
        branch += dot(normed[:, i * step : (i + 1) * step], wb[i * step : (i + 1) * step, :])
    gated = (state * jax.nn.gelu(branch)).astype(BF16)
    l_wm.wait()
    mix_s[...] = dot(gated, wm[...]).astype(BF16)

    l_sg = load(19, sg_h, sg)
    l_su = load(20, su_h, su)
    l_sd = load(21, sd_h, sd)
    l_eg = load(22, eg_h, eg)
    l_eu = load(23, eu_h, eu)
    l_ed = [load(24 + i, ed_h.at[:, pl.ds(i * HALF, HALF)], ed.at[i]) for i in range(2)]

    pl.semaphore_wait(barrier, 1 + (NZ - 1) + (NQ - 1))

    def remote(src, dst, ssem, rsem, e, t):
        return pltpu.make_async_remote_copy(
            src_ref=src, dst_ref=dst, send_sem=ssem, recv_sem=rsem, device_id=(e, t), device_id_type=MESH
        )

    mix_copy = remote(mix_s, mix_r, tp_s.at[0], tp_r.at[0], me, 1 - c)
    mix_copy.start()

    def meta_copy(i, to):
        return remote(meta_s, meta_r.at[to], ms_s.at[i], ms_r.at[to], z_peer(i) * NQ + q, c)

    def meta_send(i, carry):
        meta_copy(i, z).start()
        return carry

    lax.fori_loop(1, NZ, meta_send, 0)

    mix_copy.wait()
    mixed = mix_s[...].astype(F32) + mix_r[...].astype(F32)
    middle = (tok[...].astype(F32) + scaled(mixed, gains[1:2, :])).astype(BF16)
    middle_v[...] = middle
    ffn[...] = scaled(middle.astype(F32), gains[2:3, :]).astype(BF16)

    def z_out(ch, i):
        block = rows(z, SEQ)
        return remote(
            g_buf.at[ch, block], g_buf.at[ch, block], za_s.at[ch, i], za_r.at[ch, z], z_peer(i) * NQ + q, c
        )

    def z_in(ch, i):
        block = rows(z_peer(i), SEQ)
        return remote(
            g_buf.at[ch, block], g_buf.at[ch, block], za_s.at[ch, i], za_r.at[ch, z_peer(i)], z_peer(i) * NQ + q, c
        )

    for ch in range(NCH):
        g_buf[ch, rows(z, SEQ), :] = ffn[:, pl.ds(pl.multiple_of(c * HALF + ch * CW, CW), CW)]

        def z_send(i, carry, ch=ch):
            z_out(ch, i).start()
            return carry

        lax.fori_loop(1, NZ, z_send, 0)

    l_sg.wait()
    l_su.wait()
    l_sd.wait()
    hidden = (jax.nn.silu(dot(ffn[...], sg[...])) * dot(ffn[...], su[...])).astype(BF16)
    sh_s[...] = dot(hidden, sd[...]).astype(BF16)
    sh_copy = remote(sh_s, sh_r, tp_s.at[1], tp_r.at[1], me, 1 - c)
    sh_copy.start()

    def meta_wait(i, carry):
        meta_copy(i, z_peer(i)).wait()
        return carry

    lax.fori_loop(1, NZ, meta_wait, 0)
    meta = jnp.sum(meta_r[...], axis=0)
    code = meta[0:TOP, :].astype(jnp.int32)
    place = ((code % (2 * NQ)) // 2) * ROWS + (lane // SEQ) * 2 + code % 2
    place = jnp.where(code // (2 * NQ) == z, place, -1)
    row = lax.broadcasted_iota(jnp.int32, (NQ * ROWS, NZ * SEQ), 0)
    filled = jnp.zeros((NQ * ROWS, NZ * SEQ), F32)
    weight = jnp.zeros((NQ * ROWS, NZ * SEQ), F32)
    for k in range(TOP):
        hit = row == place[k : k + 1, :]
        filled = jnp.where(hit, 1.0, filled)
        weight = jnp.where(hit, meta[TOP + k : TOP + k + 1, :], weight)
    p_buf[...] = filled.astype(BF16)
    weight = weight.T
    high = weight.astype(BF16)
    whi[...] = high
    wlo[...] = (weight - high.astype(F32)).astype(BF16)

    def q_copy(src, dst, ss, rs, ch, i, at):
        p = q_peer(i)
        return remote(src.at[ch, rows(p, ROWS)], dst.at[rows(at, ROWS)], ss.at[ch, i], rs.at[ch, at], z * NQ + p, c)

    for ch in range(NCH):

        def z_wait(i, carry, ch=ch):
            z_in(ch, i).wait()
            return carry

        lax.fori_loop(1, NZ, z_wait, 0)
        r_buf[ch] = dot(p_buf[...], g_buf[ch]).astype(BF16)

        def q_send(i, carry, ch=ch):
            q_copy(r_buf, x_buf.at[c, ch], xa_s, xa_r, ch, i, q).start()
            return carry

        lax.fori_loop(1, NQ, q_send, 0)
        x_buf[c, ch, rows(q, ROWS), :] = r_buf[ch, rows(q, ROWS), :]

    l_eg.wait()
    l_eu.wait()
    gate = jnp.zeros((NQ * ROWS, HID), F32)
    up = jnp.zeros((NQ * ROWS, HID), F32)
    forwards = []
    for ch in range(NCH):

        def q_wait(i, carry, ch=ch):
            q_copy(r_buf, x_buf.at[c, ch], xa_s, xa_r, ch, i, q_peer(i)).wait()
            return carry

        lax.fori_loop(1, NQ, q_wait, 0)
        copy = remote(x_buf.at[c, ch], x_buf.at[c, ch], xf_s.at[ch], xf_r.at[ch], me, 1 - c)
        copy.start()
        forwards.append(copy)
        depth = rows(c * NCH + ch, CW)
        gate += dot(x_buf[c, ch], eg[0, depth, :])
        up += dot(x_buf[c, ch], eu[0, depth, :])
    for ch in range(NCH):
        other = remote(x_buf.at[1 - c, ch], x_buf.at[1 - c, ch], xf_s.at[ch], xf_r.at[ch], me, 1 - c)
        other.wait_recv()
        forwards[ch].wait_send()
        depth = rows((1 - c) * NCH + ch, CW)
        gate += dot(x_buf[1 - c, ch], eg[0, depth, :])
        up += dot(x_buf[1 - c, ch], eu[0, depth, :])
    hid_v[...] = (jax.nn.silu(gate) * up).astype(BF16)

    for copy in l_ed:
        copy.wait()
    trades = []
    for ch in range(NCH):
        y_s[ch] = dot(hid_v[...], ed[1 - c, :, ch * CW : (ch + 1) * CW]).astype(BF16)
        copy = remote(y_s.at[ch], y_r.at[ch], yx_s.at[ch], yx_r.at[ch], me, 1 - c)
        copy.start()
        trades.append(copy)
    for ch in range(NCH):
        own = dot(hid_v[...], ed[c, :, ch * CW : (ch + 1) * CW]).astype(BF16).astype(F32)
        trades[ch].wait()
        o_buf[ch] = (own + y_r[ch].astype(F32)).astype(BF16)

        def back_send(i, carry, ch=ch):
            q_copy(o_buf, b_buf.at[ch], xb_s, xb_r, ch, i, q).start()
            return carry

        lax.fori_loop(1, NQ, back_send, 0)
        b_buf[ch, rows(q, ROWS), :] = o_buf[ch, rows(q, ROWS), :]

    def sum_copy(ch, i, at):
        p = z_peer(i)
        return remote(
            t_buf.at[ch, rows(p, SEQ)], v_buf.at[ch, rows(at, SEQ)], zb_s.at[ch, i], zb_r.at[ch, at], p * NQ + q, c
        )

    for ch in range(NCH):

        def back_wait(i, carry, ch=ch):
            q_copy(o_buf, b_buf.at[ch], xb_s, xb_r, ch, i, q_peer(i)).wait()
            return carry

        lax.fori_loop(1, NQ, back_wait, 0)
        t_buf[ch] = (dot(whi[...], b_buf[ch]) + dot(wlo[...], b_buf[ch])).astype(BF16)

        def sum_send(i, carry, ch=ch):
            sum_copy(ch, i, z).start()
            return carry

        lax.fori_loop(1, NZ, sum_send, 0)
        v_buf[ch, rows(z, SEQ), :] = t_buf[ch, rows(z, SEQ), :]

    sh_copy.wait()
    shared = sh_s[...].astype(F32) + sh_r[...].astype(F32)
    pairs = []
    for ch in range(NCH):

        def sum_wait(i, carry, ch=ch):
            sum_copy(ch, i, z_peer(i)).wait()
            return carry

        lax.fori_loop(1, NZ, sum_wait, 0)
        total = v_buf[ch, 0:SEQ, :].astype(F32)
        for s in range(1, NZ):
            total += v_buf[ch, s * SEQ : (s + 1) * SEQ, :].astype(F32)
        rt_buf[c, ch] = total.astype(BF16)
        copy = remote(rt_buf.at[c, ch], rt_buf.at[c, ch], rt_s.at[ch], rt_r.at[ch], me, 1 - c)
        copy.start()
        pairs.append(copy)
    for ch in range(NCH):
        remote(rt_buf.at[1 - c, ch], rt_buf.at[1 - c, ch], rt_s.at[ch], rt_r.at[ch], me, 1 - c).wait_recv()
        pairs[ch].wait_send()
    routed = jnp.concatenate([rt_buf[h, ch] for h in range(2) for ch in range(NCH)], axis=1)
    last = scaled(routed.astype(F32) + shared, gains[3:4, :])
    out_v[...] = (middle_v[...].astype(F32) + last).astype(BF16)
    o_out = pltpu.make_async_copy(out_v, out_h, osem.at[2])
    o_out.start()
    o_inflow.wait()
    o_state.wait()
    o_out.wait()


def on_device(
    tokens, lru_state, conv_window, gain_mix_in, gain_mix_out, gain_ffn_in, gain_ffn_out, w_branch, w_input,
    conv_taps, gate_a, gate_x, decay_rate, w_mix_out, routes, route_weight, expert_gate, expert_up, expert_down,
    shared_gate, shared_up, shared_down,
):
    taps = conv_taps.astype(F32)
    convp = jnp.sum(conv_window.astype(F32) * taps[None, :3], axis=1)
    gains = jnp.stack([gain_mix_in, gain_mix_out, gain_ffn_in, gain_ffn_out])
    meta = jnp.tile(jnp.concatenate([routes.astype(F32), route_weight], axis=1).T, (1, NZ))
    hbm = pl.BlockSpec(memory_space=pltpu.HBM)

    def vmem(*shape, dtype=BF16):
        return pltpu.VMEM(shape, dtype)

    def dma(*shape):
        return pltpu.SemaphoreType.DMA(shape)

    scratch = [
        vmem(SEQ, D), vmem(SEQ, LC, dtype=F32), vmem(SEQ, LC, dtype=F32), vmem(4, LC), vmem(4, D, dtype=F32),
        vmem(1, LC, dtype=F32), vmem(D, LC), vmem(D, LC), vmem(4, 128, 128), vmem(4, 128, 128), vmem(LC, D),
        vmem(SEQ, TOP, dtype=jnp.int32), vmem(2 * TOP, NZ * SEQ, dtype=F32),
        vmem(1, D, HID), vmem(1, D, HID), vmem(2, HID, HALF), vmem(D, HID), vmem(D, HID), vmem(HID, D),
        vmem(SEQ, LC, dtype=F32), vmem(SEQ, LC), vmem(SEQ, D), vmem(SEQ, D), vmem(SEQ, D),
        vmem(SEQ, D), vmem(SEQ, D), vmem(2 * TOP, NZ * SEQ, dtype=F32), vmem(NZ, 2 * TOP, NZ * SEQ, dtype=F32),
        vmem(SEQ, D), vmem(SEQ, D),
        vmem(NCH, NZ * SEQ, CW), vmem(NCH, NQ * ROWS, CW), vmem(2, NCH, NQ * ROWS, CW),
        vmem(NQ * ROWS, NZ * SEQ), vmem(NZ * SEQ, NQ * ROWS), vmem(NZ * SEQ, NQ * ROWS), vmem(NQ * ROWS, HID),
        vmem(NCH, NQ * ROWS, CW), vmem(NCH, NQ * ROWS, CW), vmem(NCH, NQ * ROWS, CW), vmem(NCH, NQ * ROWS, CW),
        vmem(NCH, NZ * SEQ, CW), vmem(NCH, NZ * SEQ, CW), vmem(2, NCH, SEQ, CW),
        dma(26), dma(3),
        dma(2), dma(2), dma(NZ), dma(NZ), dma(NCH, NZ), dma(NCH, NZ), dma(NCH, NQ), dma(NCH, NQ), dma(NCH), dma(NCH),
        dma(NCH), dma(NCH), dma(NCH, NQ), dma(NCH, NQ), dma(NCH, NZ), dma(NCH, NZ), dma(NCH), dma(NCH),
    ]
    layer_out, new_state, inflow = pl.pallas_call(
        kernel,
        out_shape=(
            jax.ShapeDtypeStruct((SEQ, D), BF16),
            jax.ShapeDtypeStruct((SEQ, LC), F32),
            jax.ShapeDtypeStruct((SEQ, LC), BF16),
        ),
        in_specs=[hbm] * 19,
        out_specs=(hbm,) * 3,
        scratch_shapes=scratch,
        compiler_params=pltpu.CompilerParams(collective_id=0, has_side_effects=True, vmem_limit_bytes=60 * 2**20),
        name="layer",
    )(
        tokens, lru_state, convp, conv_taps, gains, decay_rate[None], w_branch, w_input, gate_a, gate_x, w_mix_out,
        routes, meta, expert_gate, expert_up, expert_down[0], shared_gate, shared_up, shared_down,
    )
    new_window = jnp.concatenate([conv_window[:, 1:], inflow[:, None, :]], axis=1)
    return (layer_out, new_state, new_window)


def solution(mesh):
    placed = (
        P("ep", None),
        P("ep", "tp"),
        P("ep", None, "tp"),
        P(),
        P(),
        P(),
        P(),
        P(None, "tp"),
        P(None, "tp"),
        P(None, "tp"),
        P("tp", None, None),
        P("tp", None, None),
        P("tp"),
        P("tp", None),
        P("ep", None),
        P("ep", None),
        P("ep", None, "tp"),
        P("ep", None, "tp"),
        P("ep", "tp", None),
        P(None, "tp"),
        P(None, "tp"),
        P("tp", None),
    )
    return jax.shard_map(
        on_device,
        mesh=mesh,
        in_specs=placed,
        out_specs=(P("ep", None), P("ep", "tp"), P("ep", None, "tp")),
        check_vma=False,
    )
```

time: 117 us -> 73.8 us (0.63)
  Pallas kernels: 0 us -> 61.2 us
  blocking collectives: 56.9 us -> 0 us
  matrix products: 14.6 us -> 0 us
  waiting for transfers between devices: 12.5 us -> 0 us
  local copies, waits for them, and re-layouts: 13.9 us -> 5.08 us
  starting transfers between devices: 6.17 us -> 0 us
  other arithmetic: 10.6 us -> 6.42 us
    pallas_call x0 -> x1, Pallas kernels: none -> 61.2 us  [on_device(): pl.pallas_call(kernel, out_shape=(jax.ShapeDtypeStruct((SEQ, D), BF16), j...]
    all_to_all x4 -> x0, blocking collectives: 50.1 us -> none  [the longest x1 32.4 us: on_device(): arrived = lax.all_to_all(own, 'ep', split_axis=0, concat_axis=1, tiled=True)]
    dot_general x9 -> x0, matrix products: 14.6 us -> none  [the longest x1 3.93 us: on_device(): jnp.einsum('erf,efd->erd', hidden, expert_down, preferred_element_type=jn...]
    all_to_all x1 -> x0, waiting for transfers between devices: 12.5 us -> none  [on_device(): back = lax.all_to_all(summed, 'ep', split_axis=1, concat_axis=0, tiled=True)]
    all_gather x2 -> x0, blocking collectives: 6.83 us -> none  [gathered_total(): blocks = lax.all_gather(array, axis).astype(jnp.float32)]
    all_to_all x1 -> x0, starting transfers between devices: 6.17 us -> none  [on_device(): back = lax.all_to_all(summed, 'ep', split_axis=1, concat_axis=0, tiled=True)]
    unnamed x2 -> x0, other arithmetic: 4.52 us -> none
    reshape x2 -> x0, local copies, waits for them, and re-layouts: 2.82 us -> none  [the longest x1 1.52 us: on_device(): outbound = outbound.astype(jnp.bfloat16).reshape(experts, capacity, width)]
  transfers between devices with their start and end apart: 1 -> 0, of which waited for: 1 -> 0; matrix products, arithmetic and copies ran while one was open for 4% -> 0% of each run, Pallas kernels for 0% -> 0%
where the time goes in v1:
time: 73.8 us; the launch traced here: 73.4 us
  Pallas kernels  61.2 us (83%)
  other arithmetic  6.42 us (9%)
  local copies, waits for them, and re-layouts  5.08 us (7%)
    pallas_call x1, Pallas kernels, on_device(): pl.pallas_call(kernel, out_shape=(jax.ShapeDtypeStruct((SEQ, D), BF16), j...  61.2 us
    unnamed x3, local copies, waits for them, and re-layouts  4.41 us
    reduce_sum x1, other arithmetic, on_device(): convp = jnp.sum(conv_window.astype(F32) * taps[None, :3], axis=1)  1.55 us

profile of v1, /device:TPU:1, one launch (start us, length us, event | category | flops | bytes accessed | tf_op | source)
XLA Modules:
  0.0 73.4 jit_solution(654424674280640110)
XLA Ops:
  0.6 0.7 slice_convert_fusion
  1.3 1.5 %multiply_reduce_fusion.convp_h = f32[32,512]{1,0:T(8,128)} fusion(bf16[32,3,512]{2,0,1:T(8,128)(2,1)} %param.24, f32[3,512]{1,0:T(4,128)S(1)} %slice_convert_fusion), kind=kLoop, calls=%fused_computation | loop fusion | flops 131072 | bytes 169984 | tf_op jit(solution)/shard_map/reduce_sum | solution.py:359
  2.9 1.4 %pad_maximum_fusion.1.gains_h = f32[4,2048]{1,0:T(4,128)} fusion(f32[1,2048]{1,0:T(1,128)} %bitcast.11, f32[1,2048]{1,0:T(1,128)} %bitcast.12, f32[1,2048]{1,0:T(1,128)} %bitcast.13, f32[1,2048]{1,0:T(1,128)} %bitcast.14), kind=kLoop, calls=%fused_computation.2 | loop fusion | flops 24576 | bytes 65536 | tf_op jit(solution)/shard_map/stack | solution.py:360
  4.3 1.4 %copy.25.routes_h = s32[32,4]{1,0:T(8,128)} copy(s32[32,4]{0,1:T(4,128)} %param.36) | data formatting | bytes 1024 | tf_op args[14]
  5.6 0.7 convert_element_type.8
  6.3 0.7 maximum_bitcast_fusion
  7.0 0.7 tile.10.meta_h
  7.7 0.0 slice-start
  7.7 61.2 %layer.1 = (bf16[32,2048]{1,0:T(8,128)(2,1)}, f32[32,512]{1,0:T(8,128)}, bf16[32,512]{1,0:T(8,128)(2,1)}) custom-call(bf16[32,2048]{1,0:T(8,128)(2,1)} %tok_h.1, f32[32,512]{1,0:T(8,128)} %lru_h.1, f32[32,512]{1,0:T(8,128)} %multiply_reduce_fusion.convp_h, bf16[4,512]{1,0:T(4,128)(2,1)} %taps_h.1, f32[4,2048]{1,0:T(4,128)} %pad_maximum_fusion.1.gains_h, ...), custom_call_target="tpu_custom_call" | custom-call | tf_op jit(solution)/shard_map/layer/pallas_call | solution.py:386
  68.9 0.0 slice-done
  68.9 1.4 %pad_maximum_fusion = bf16[32,3,512]{2,0,1:T(8,128)(2,1)} fusion(bf16[32,1,512]{2,0,1:T(8,128)(2,1)} %bitcast.10, bf16[32,2,512]{2,0,1:T(8,128)(2,1)S(1)} %slice-done), kind=kLoop, calls=%fused_computation.1 | loop fusion | flops 49152 | bytes 196608 | tf_op jit(solution)/shard_map/concatenate | solution.py:402
  70.3 1.6 %copy.28 = bf16[32,2048]{1,0:T(8,128)(2,1)} copy(bf16[32,2048]{1,0:T(8,128)(2,1)} %get-tuple-element.12) | data formatting | bytes 262144
  71.9 1.5 %copy.29 = f32[32,512]{1,0:T(8,128)} copy(f32[32,512]{1,0:T(8,128)} %get-tuple-element.13) | data formatting | bytes 131072
  (1 shorter events, 0.0 us)
Async XLA Ops:
  7.7 61.2 %slice-start = ((bf16[32,3,512]{2,0,1:T(8,128)(2,1)}), bf16[32,2,512]{2,0,1:T(8,128)(2,1)S(1)}, s32[]{:S(2)}) async-start(bf16[32,3,512]{2,0,1:T(8,128)(2,1)} %param.24), calls=%async_computation | async-start | bytes 131072 | tf_op jit(solution)/shard_map/slice | solution.py:402

commit v2 on v1

--- a/solution.py
+++ b/solution.py
@@ -34,15 +34,15 @@
 
 
 def kernel(
-    tok_h, lru_h, convp_h, taps_h, gains_h, decay_h, wb_h, wi_h, ga_h, gx_h, wm_h, routes_h, meta_h,
-    eg_h, eu_h, ed_h, sg_h, su_h, sd_h,
-    out_h, state_h, inflow_h,
-    tok, lru, convp, taps, gains, decay, wb, wi, ga, gx, wm, routes, meta_in,
+    tok_h, lru_h, win_h, taps_h, gain0_h, gain1_h, gain2_h, gain3_h, decay_h, wb_h, wi_h, ga_h, gx_h, wm_h,
+    routes_h, rweight_h, eg_h, eu_h, ed_h, sg_h, su_h, sd_h,
+    out_v, state_v, window_v,
+    tok, lru, win, taps, gains, decay, wb, wi, ga, gx, wm, routes, rweight,
     eg, eu, ed, sg, su, sd,
-    state_v, inflow_v, out_v, middle_v, ffn,
+    middle_v, ffn,
     mix_s, mix_r, meta_s, meta_r, sh_s, sh_r,
     g_buf, r_buf, x_buf, p_buf, whi, wlo, hid_v, y_s, y_r, o_buf, b_buf, t_buf, v_buf, rt_buf,
-    lsem, osem,
+    lsem,
     tp_s, tp_r, ms_s, ms_r, za_s, za_r, xa_s, xa_r, xf_s, xf_r, yx_s, yx_r, xb_s, xb_r, zb_s, zb_r, rt_s, rt_r,
 ):
     me = lax.axis_index("ep")
@@ -81,49 +81,56 @@
 
     step = D // NPIECE
     l_tok = load(0, tok_h, tok)
-    l_gains = load(1, gains_h, gains)
-    l_wi = [load(2 + i, wi_h.at[pl.ds(i * step, step)], wi.at[pl.ds(i * step, step)]) for i in range(NPIECE)]
-    l_convp = load(6, convp_h, convp)
-    l_taps = load(7, taps_h, taps)
-    l_ga = load(8, ga_h, ga)
-    l_gx = load(9, gx_h, gx)
-    l_wb = [load(10 + i, wb_h.at[pl.ds(i * step, step)], wb.at[pl.ds(i * step, step)]) for i in range(NPIECE)]
-    l_decay = load(14, decay_h, decay)
-    l_lru = load(15, lru_h, lru)
-    l_routes = load(16, routes_h, routes)
-    l_meta = load(17, meta_h, meta_in)
-    l_wm = load(18, wm_h, wm)
-
-    l_routes.wait()
-    l_meta.wait()
-    lane = lax.broadcasted_iota(jnp.int32, (1, NZ * SEQ), 1)
-    mine = (lane // SEQ) == z
-    earlier = lax.broadcasted_iota(jnp.int32, (SEQ, NZ * SEQ), 0) < (lane % SEQ)
-    named = routes[...].astype(F32)
-    for k in range(TOP):
-        expert = meta_in[k : k + 1, :]
-        same = named[:, 0:1] == expert
-        for j in range(1, TOP):
-            same = same | (named[:, j : j + 1] == expert)
-        rank = jnp.sum(jnp.where(same & earlier, 1.0, 0.0), axis=0, keepdims=True)
-        meta_s[k : k + 1, :] = jnp.where(mine, 2.0 * expert + rank, 0.0)
-    meta_s[TOP : 2 * TOP, :] = jnp.where(mine, meta_in[TOP : 2 * TOP, :], 0.0)
-    meta_r[pl.ds(z, 1)] = meta_s[...][None]
+    l_gains = [load(1 + i, h, gains.at[i]) for i, h in enumerate((gain0_h, gain1_h, gain2_h, gain3_h))]
+    l_wi = [load(5 + i, wi_h.at[pl.ds(i * step, step)], wi.at[pl.ds(i * step, step)]) for i in range(NPIECE)]
+    l_win = load(9, win_h, win)
+    l_taps = load(10, taps_h, taps)
+    l_ga = load(11, ga_h, ga)
+    l_gx = load(12, gx_h, gx)
+    l_routes = load(13, routes_h, routes)
+    l_rweight = load(14, rweight_h, rweight)
+    l_wb = [load(15 + i, wb_h.at[pl.ds(i * step, step)], wb.at[pl.ds(i * step, step)]) for i in range(NPIECE)]
+    l_decay = load(19, decay_h, decay)
+    l_lru = load(20, lru_h, lru)
+    l_wm = load(21, wm_h, wm)
+
+    with jax.named_scope("slots"):
+        l_routes.wait()
+        l_rweight.wait()
+        lane = lax.broadcasted_iota(jnp.int32, (1, NZ * SEQ), 1)
+        mine = (lane // SEQ) == z
+        earlier = lax.broadcasted_iota(jnp.int32, (SEQ, NZ * SEQ), 0) < (lane % SEQ)
+        diagonal = lax.broadcasted_iota(jnp.int32, (SEQ, SEQ), 0) == lax.broadcasted_iota(jnp.int32, (SEQ, SEQ), 1)
+        narrow = routes[...].astype(F32)
+        named = [
+            jnp.sum(jnp.where(diagonal, narrow[k : k + 1, :], 0.0), axis=1, keepdims=True) for k in range(TOP)
+        ]
+        wide = jnp.concatenate([narrow] * NZ, axis=1)
+        for k in range(TOP):
+            expert = wide[k : k + 1, :]
+            same = named[0] == expert
+            for j in range(1, TOP):
+                same = same | (named[j] == expert)
+            rank = jnp.sum(jnp.where(same & earlier, 1.0, 0.0), axis=0, keepdims=True)
+            meta_s[k : k + 1, :] = jnp.where(mine, 2.0 * expert + rank, 0.0)
+        meta_s[TOP : 2 * TOP, :] = jnp.where(mine, jnp.concatenate([rweight[...]] * NZ, axis=1), 0.0)
+        meta_r[pl.ds(z, 1)] = meta_s[...][None]
 
     l_tok.wait()
-    l_gains.wait()
-    normed = scaled(tok[...].astype(F32), gains[0:1, :]).astype(BF16)
+    for copy in l_gains:
+        copy.wait()
+    normed = scaled(tok[...].astype(F32), gains[0]).astype(BF16)
     inflow = jnp.zeros((SEQ, LC), F32)
     for i in range(NPIECE):
         l_wi[i].wait()
         inflow += dot(normed[:, i * step : (i + 1) * step], wi[i * step : (i + 1) * step, :])
     inflow = inflow.astype(BF16)
-    inflow_v[...] = inflow
-    o_inflow = pltpu.make_async_copy(inflow_v, inflow_h, osem.at[0])
-    o_inflow.start()
-    l_convp.wait()
+    l_win.wait()
     l_taps.wait()
-    conv = convp[...] + inflow.astype(F32) * taps[3:4, :].astype(F32)
+    conv = inflow.astype(F32) * taps[3:4, :].astype(F32)
+    for j in range(3):
+        conv += win[j].astype(F32) * taps[j : j + 1, :].astype(F32)
+        window_v[j] = win[j + 1] if j < 2 else inflow
     low = conv.astype(BF16)
     l_ga.wait()
     l_gx.wait()
@@ -138,8 +145,6 @@
     t = jnp.tanh(fall)
     state = jnp.exp(-fall) * lru[...] + jnp.sqrt(2.0 * t / (1.0 + t)) * conv * input_gate
     state_v[...] = state
-    o_state = pltpu.make_async_copy(state_v, state_h, osem.at[1])
-    o_state.start()
     branch = jnp.zeros((SEQ, LC), F32)
     for i in range(NPIECE):
         l_wb[i].wait()
@@ -148,12 +153,12 @@
     l_wm.wait()
     mix_s[...] = dot(gated, wm[...]).astype(BF16)
 
-    l_sg = load(19, sg_h, sg)
-    l_su = load(20, su_h, su)
-    l_sd = load(21, sd_h, sd)
-    l_eg = load(22, eg_h, eg)
-    l_eu = load(23, eu_h, eu)
-    l_ed = [load(24 + i, ed_h.at[:, pl.ds(i * HALF, HALF)], ed.at[i]) for i in range(2)]
+    l_sg = load(22, sg_h, sg)
+    l_su = load(23, su_h, su)
+    l_sd = load(24, sd_h, sd)
+    l_eg = load(25, eg_h, eg)
+    l_eu = load(26, eu_h, eu)
+    l_ed = [load(27 + i, ed_h.at[:, pl.ds(i * HALF, HALF)], ed.at[i]) for i in range(2)]
 
     pl.semaphore_wait(barrier, 1 + (NZ - 1) + (NQ - 1))
 
@@ -176,9 +181,9 @@
 
     mix_copy.wait()
     mixed = mix_s[...].astype(F32) + mix_r[...].astype(F32)
-    middle = (tok[...].astype(F32) + scaled(mixed, gains[1:2, :])).astype(BF16)
+    middle = (tok[...].astype(F32) + scaled(mixed, gains[1])).astype(BF16)
     middle_v[...] = middle
-    ffn[...] = scaled(middle.astype(F32), gains[2:3, :]).astype(BF16)
+    ffn[...] = scaled(middle.astype(F32), gains[2]).astype(BF16)
 
     def z_out(ch, i):
         block = rows(z, SEQ)
@@ -341,13 +346,17 @@
         remote(rt_buf.at[1 - c, ch], rt_buf.at[1 - c, ch], rt_s.at[ch], rt_r.at[ch], me, 1 - c).wait_recv()
         pairs[ch].wait_send()
     routed = jnp.concatenate([rt_buf[h, ch] for h in range(2) for ch in range(NCH)], axis=1)
-    last = scaled(routed.astype(F32) + shared, gains[3:4, :])
+    last = scaled(routed.astype(F32) + shared, gains[3])
     out_v[...] = (middle_v[...].astype(F32) + last).astype(BF16)
-    o_out = pltpu.make_async_copy(out_v, out_h, osem.at[2])
-    o_out.start()
-    o_inflow.wait()
-    o_state.wait()
-    o_out.wait()
+
+
+def store(*refs):
+    n = len(refs) // 2
+    copies = [pltpu.make_async_copy(refs[i], refs[n + i], refs[-1].at[i]) for i in range(n)]
+    for copy in copies:
+        copy.start()
+    for copy in copies:
+        copy.wait()
 
 
 def on_device(
@@ -355,10 +364,6 @@
     conv_taps, gate_a, gate_x, decay_rate, w_mix_out, routes, route_weight, expert_gate, expert_up, expert_down,
     shared_gate, shared_up, shared_down,
 ):
-    taps = conv_taps.astype(F32)
-    convp = jnp.sum(conv_window.astype(F32) * taps[None, :3], axis=1)
-    gains = jnp.stack([gain_mix_in, gain_mix_out, gain_ffn_in, gain_ffn_out])
-    meta = jnp.tile(jnp.concatenate([routes.astype(F32), route_weight], axis=1).T, (1, NZ))
     hbm = pl.BlockSpec(memory_space=pltpu.HBM)
 
     def vmem(*shape, dtype=BF16):
@@ -368,39 +373,49 @@
         return pltpu.SemaphoreType.DMA(shape)
 
     scratch = [
-        vmem(SEQ, D), vmem(SEQ, LC, dtype=F32), vmem(SEQ, LC, dtype=F32), vmem(4, LC), vmem(4, D, dtype=F32),
+        vmem(SEQ, D), vmem(SEQ, LC, dtype=F32), vmem(3, SEQ, LC), vmem(4, LC), vmem(4, 1, D, dtype=F32),
         vmem(1, LC, dtype=F32), vmem(D, LC), vmem(D, LC), vmem(4, 128, 128), vmem(4, 128, 128), vmem(LC, D),
-        vmem(SEQ, TOP, dtype=jnp.int32), vmem(2 * TOP, NZ * SEQ, dtype=F32),
+        vmem(TOP, SEQ, dtype=jnp.int32), vmem(TOP, SEQ, dtype=F32),
         vmem(1, D, HID), vmem(1, D, HID), vmem(2, HID, HALF), vmem(D, HID), vmem(D, HID), vmem(HID, D),
-        vmem(SEQ, LC, dtype=F32), vmem(SEQ, LC), vmem(SEQ, D), vmem(SEQ, D), vmem(SEQ, D),
+        vmem(SEQ, D), vmem(SEQ, D),
         vmem(SEQ, D), vmem(SEQ, D), vmem(2 * TOP, NZ * SEQ, dtype=F32), vmem(NZ, 2 * TOP, NZ * SEQ, dtype=F32),
         vmem(SEQ, D), vmem(SEQ, D),
         vmem(NCH, NZ * SEQ, CW), vmem(NCH, NQ * ROWS, CW), vmem(2, NCH, NQ * ROWS, CW),
         vmem(NQ * ROWS, NZ * SEQ), vmem(NZ * SEQ, NQ * ROWS), vmem(NZ * SEQ, NQ * ROWS), vmem(NQ * ROWS, HID),
         vmem(NCH, NQ * ROWS, CW), vmem(NCH, NQ * ROWS, CW), vmem(NCH, NQ * ROWS, CW), vmem(NCH, NQ * ROWS, CW),
         vmem(NCH, NZ * SEQ, CW), vmem(NCH, NZ * SEQ, CW), vmem(2, NCH, SEQ, CW),
-        dma(26), dma(3),
+        dma(29),
         dma(2), dma(2), dma(NZ), dma(NZ), dma(NCH, NZ), dma(NCH, NZ), dma(NCH, NQ), dma(NCH, NQ), dma(NCH), dma(NCH),
         dma(NCH), dma(NCH), dma(NCH, NQ), dma(NCH, NQ), dma(NCH, NZ), dma(NCH, NZ), dma(NCH), dma(NCH),
     ]
-    layer_out, new_state, inflow = pl.pallas_call(
+    vm = pl.BlockSpec(memory_space=pltpu.VMEM)
+    results = pl.pallas_call(
         kernel,
         out_shape=(
-            jax.ShapeDtypeStruct((SEQ, D), BF16),
-            jax.ShapeDtypeStruct((SEQ, LC), F32),
-            jax.ShapeDtypeStruct((SEQ, LC), BF16),
+            pltpu.VMEM((SEQ, D), BF16),
+            pltpu.VMEM((SEQ, LC), F32),
+            pltpu.VMEM((3, SEQ, LC), BF16),
         ),
-        in_specs=[hbm] * 19,
-        out_specs=(hbm,) * 3,
+        in_specs=[hbm] * 22,
+        out_specs=(vm,) * 3,
         scratch_shapes=scratch,
         compiler_params=pltpu.CompilerParams(collective_id=0, has_side_effects=True, vmem_limit_bytes=60 * 2**20),
         name="layer",
     )(
-        tokens, lru_state, convp, conv_taps, gains, decay_rate[None], w_branch, w_input, gate_a, gate_x, w_mix_out,
-        routes, meta, expert_gate, expert_up, expert_down[0], shared_gate, shared_up, shared_down,
+        tokens, lru_state, conv_window.transpose(1, 0, 2), conv_taps, gain_mix_in[None], gain_mix_out[None],
+        gain_ffn_in[None], gain_ffn_out[None], decay_rate[None], w_branch, w_input, gate_a, gate_x, w_mix_out,
+        routes.T, route_weight.T, expert_gate, expert_up, expert_down[0], shared_gate, shared_up, shared_down,
     )
-    new_window = jnp.concatenate([conv_window[:, 1:], inflow[:, None, :]], axis=1)
-    return (layer_out, new_state, new_window)
+    layer_out, new_state, window = pl.pallas_call(
+        store,
+        out_shape=tuple(jax.ShapeDtypeStruct(r.shape, r.dtype) for r in results),
+        in_specs=[vm] * 3,
+        out_specs=(hbm,) * 3,
+        scratch_shapes=[dma(3)],
+        compiler_params=pltpu.CompilerParams(has_side_effects=True, vmem_limit_bytes=2**20),
+        name="store",
+    )(*results)
+    return (layer_out, new_state, window.transpose(1, 0, 2))
 
 
 def solution(mesh):

time: 73.8 us -> 61.2 us (0.83)
  other arithmetic: 6.42 us -> 0 us
  local copies, waits for them, and re-layouts: 5.08 us -> 0 us
    unnamed x3 -> x0, local copies, waits for them, and re-layouts: 4.41 us -> none
    reduce_sum x1 -> x0, other arithmetic: 1.55 us -> none  [on_device(): convp = jnp.sum(conv_window.astype(F32) * taps[None, :3], axis=1)]
    concatenate x1 -> x0, other arithmetic: 1.41 us -> none  [on_device(): jnp.concatenate([conv_window[:, 1:], inflow[:, None, :]], axis=1)]
    another operation x1 -> x0, other arithmetic: 1.4 us -> none  [on_device(): gains = jnp.stack([gain_mix_in, gain_mix_out, gain_ffn_in, gain_ffn_out])]
    pallas_call x1 -> x2, Pallas kernels: 61.2 us -> 60.5 us  [the longest x1 59.7 us: on_device(): pl.pallas_call(kernel, out_shape=(pltpu.VMEM((SEQ, D), BF16), pltpu.VMEM(...]
where the time goes in v2:
time: 61.2 us; the launch traced here: 61.1 us
  Pallas kernels  60.5 us (99%)
  between operations  0.65 us (1%)
    pallas_call x1, Pallas kernels, on_device(): pl.pallas_call(kernel, out_shape=(pltpu.VMEM((SEQ, D), BF16), pltpu.VMEM(...  59.7 us

profile of v2, /device:TPU:1, one launch (start us, length us, event | category | flops | bytes accessed | tf_op | source)
XLA Modules:
  0.0 61.1 jit_solution(9447488035206185847)
XLA Ops:
  0.6 59.7 %layer.1 = (bf16[32,2048]{1,0:T(8,128)(2,1)S(1)}, f32[32,512]{1,0:T(8,128)S(1)}, bf16[3,32,512]{2,1,0:T(8,128)(2,1)S(1)}) custom-call(bf16[32,2048]{1,0:T(8,128)(2,1)} %tok_h.1, f32[32,512]{1,0:T(8,128)} %lru_h.1, bf16[3,32,512]{2,1,0:T(8,128)(2,1)} %bitcast.11, bf16[4,512]{1,0:T(4,128)(2,1)} %taps_h.1, f32[1,2048]{1,0:T(1,128)} %bitcast.12, ...), custom_call_target="tpu_custom_call" | custom-call | tf_op jit(solution)/shard_map/layer/pallas_call | solution.py:392
  60.4 0.7 %store.1 = (bf16[32,2048]{1,0:T(8,128)(2,1)}, f32[32,512]{1,0:T(8,128)}, bf16[3,32,512]{2,1,0:T(8,128)(2,1)}) custom-call(bf16[32,2048]{1,0:T(8,128)(2,1)S(1)} %get-tuple-element.9.refs_0_, f32[32,512]{1,0:T(8,128)S(1)} %get-tuple-element.10.refs_1_, bf16[3,32,512]{2,1,0:T(8,128)(2,1)S(1)} %get-tuple-element.11.refs_2_), custom_call_target="tpu_custom_call" | custom-call | tf_op jit(solution)/shard_map/store/pallas_call | solution.py:409

commit v3 on v2

--- a/solution.py
+++ b/solution.py
@@ -17,7 +17,7 @@
 TOP = 4
 D = 2048
 HALF = D // 2
-NCH = 2
+NCH = 4
 CW = HALF // NCH
 LC = 512
 HID = 256
@@ -41,9 +41,10 @@
     eg, eu, ed, sg, su, sd,
     middle_v, ffn,
     mix_s, mix_r, meta_s, meta_r, sh_s, sh_r,
-    g_buf, r_buf, x_buf, p_buf, whi, wlo, hid_v, y_s, y_r, o_buf, b_buf, t_buf, v_buf, rt_buf,
+    g_buf, r_buf, x_buf, p_buf, whi, wlo, hid_v, y_s, y_r, o_buf, b_buf, t_buf, rl_buf, c_buf, v_buf, rt_buf,
     lsem,
-    tp_s, tp_r, ms_s, ms_r, za_s, za_r, xa_s, xa_r, xf_s, xf_r, yx_s, yx_r, xb_s, xb_r, zb_s, zb_r, rt_s, rt_r,
+    tp_s, tp_r, ms_s, ms_r, za_s, za_two, za_r, xa_s, xa_r, xf_s, xf_r, yx_s, yx_r, xb_s, xb_r,
+    zb_s, zb_two, zb_r, rt_s, rt_r,
 ):
     me = lax.axis_index("ep")
     c = lax.axis_index("tp")
@@ -52,7 +53,7 @@
     y, x = q // 4, q % 4
 
     def z_peer(i):
-        return lax.rem(z + i, NZ)
+        return lax.rem(z + (i + NZ), NZ)
 
     def q_peer(i):
         return lax.rem(y + i // 4, 4) * 4 + lax.rem(x + i % 4, 4)
@@ -93,28 +94,6 @@
     l_decay = load(19, decay_h, decay)
     l_lru = load(20, lru_h, lru)
     l_wm = load(21, wm_h, wm)
-
-    with jax.named_scope("slots"):
-        l_routes.wait()
-        l_rweight.wait()
-        lane = lax.broadcasted_iota(jnp.int32, (1, NZ * SEQ), 1)
-        mine = (lane // SEQ) == z
-        earlier = lax.broadcasted_iota(jnp.int32, (SEQ, NZ * SEQ), 0) < (lane % SEQ)
-        diagonal = lax.broadcasted_iota(jnp.int32, (SEQ, SEQ), 0) == lax.broadcasted_iota(jnp.int32, (SEQ, SEQ), 1)
-        narrow = routes[...].astype(F32)
-        named = [
-            jnp.sum(jnp.where(diagonal, narrow[k : k + 1, :], 0.0), axis=1, keepdims=True) for k in range(TOP)
-        ]
-        wide = jnp.concatenate([narrow] * NZ, axis=1)
-        for k in range(TOP):
-            expert = wide[k : k + 1, :]
-            same = named[0] == expert
-            for j in range(1, TOP):
-                same = same | (named[j] == expert)
-            rank = jnp.sum(jnp.where(same & earlier, 1.0, 0.0), axis=0, keepdims=True)
-            meta_s[k : k + 1, :] = jnp.where(mine, 2.0 * expert + rank, 0.0)
-        meta_s[TOP : 2 * TOP, :] = jnp.where(mine, jnp.concatenate([rweight[...]] * NZ, axis=1), 0.0)
-        meta_r[pl.ds(z, 1)] = meta_s[...][None]
 
     l_tok.wait()
     for copy in l_gains:
@@ -151,7 +130,8 @@
         branch += dot(normed[:, i * step : (i + 1) * step], wb[i * step : (i + 1) * step, :])
     gated = (state * jax.nn.gelu(branch)).astype(BF16)
     l_wm.wait()
-    mix_s[...] = dot(gated, wm[...]).astype(BF16)
+    for i in range(2):
+        mix_s[i] = dot(gated, wm[:, i * HALF : (i + 1) * HALF]).astype(BF16)
 
     l_sg = load(22, sg_h, sg)
     l_su = load(23, su_h, su)
@@ -167,58 +147,83 @@
             src_ref=src, dst_ref=dst, send_sem=ssem, recv_sem=rsem, device_id=(e, t), device_id_type=MESH
         )
 
-    mix_copy = remote(mix_s, mix_r, tp_s.at[0], tp_r.at[0], me, 1 - c)
-    mix_copy.start()
-
-    def meta_copy(i, to):
-        return remote(meta_s, meta_r.at[to], ms_s.at[i], ms_r.at[to], z_peer(i) * NQ + q, c)
+    def to_z(src, dst, ssem, rsem, i):
+        return remote(src, dst, ssem, rsem, z_peer(i) * NQ + q, c)
+
+    def to_core(src, dst, ssem, rsem):
+        return remote(src, dst, ssem, rsem, me, 1 - c)
+
+    mix_copies = [to_core(mix_s.at[i], mix_r.at[i], tp_s.at[i], tp_r.at[i]) for i in range(2)]
+    for copy in mix_copies:
+        copy.start()
+
+    with jax.named_scope("slots"):
+        l_routes.wait()
+        l_rweight.wait()
+        lane = lax.broadcasted_iota(jnp.int32, (1, NZ * SEQ), 1)
+        mine = (lane // SEQ) == z
+        earlier = lax.broadcasted_iota(jnp.int32, (SEQ, NZ * SEQ), 0) < (lane % SEQ)
+        diagonal = lax.broadcasted_iota(jnp.int32, (SEQ, SEQ), 0) == lax.broadcasted_iota(jnp.int32, (SEQ, SEQ), 1)
+        narrow = routes[...].astype(F32)
+        named = [
+            jnp.sum(jnp.where(diagonal, narrow[k : k + 1, :], 0.0), axis=1, keepdims=True) for k in range(TOP)
+        ]
+        wide = jnp.concatenate([narrow] * NZ, axis=1)
+        for k in range(TOP):
+            expert = wide[k : k + 1, :]
+            same = named[0] == expert
+            for j in range(1, TOP):
+                same = same | (named[j] == expert)
+            rank = jnp.sum(jnp.where(same & earlier, 1.0, 0.0), axis=0, keepdims=True)
+            meta_s[k : k + 1, :] = jnp.where(mine, 2.0 * expert + rank, 0.0)
+        meta_s[TOP : 2 * TOP, :] = jnp.where(mine, jnp.concatenate([rweight[...]] * NZ, axis=1), 0.0)
+        meta_r[pl.ds(z, 1)] = meta_s[...][None]
 
     def meta_send(i, carry):
-        meta_copy(i, z).start()
+        to_z(meta_s, meta_r.at[z], ms_s, ms_r, i).start()
         return carry
 
     lax.fori_loop(1, NZ, meta_send, 0)
 
-    mix_copy.wait()
-    mixed = mix_s[...].astype(F32) + mix_r[...].astype(F32)
+    mixed = []
+    for i in range(2):
+        mix_copies[i].wait()
+        mixed.append(mix_s[i].astype(F32) + mix_r[i].astype(F32))
+    mixed = jnp.concatenate(mixed, axis=1)
     middle = (tok[...].astype(F32) + scaled(mixed, gains[1])).astype(BF16)
     middle_v[...] = middle
     ffn[...] = scaled(middle.astype(F32), gains[2]).astype(BF16)
 
-    def z_out(ch, i):
-        block = rows(z, SEQ)
-        return remote(
-            g_buf.at[ch, block], g_buf.at[ch, block], za_s.at[ch, i], za_r.at[ch, z], z_peer(i) * NQ + q, c
-        )
-
-    def z_in(ch, i):
-        block = rows(z_peer(i), SEQ)
-        return remote(
-            g_buf.at[ch, block], g_buf.at[ch, block], za_s.at[ch, i], za_r.at[ch, z_peer(i)], z_peer(i) * NQ + q, c
-        )
+    def z_copy(ch, source, i, rsem):
+        block = g_buf.at[ch, rows(source, SEQ)]
+        return to_z(block, block, za_s.at[ch], rsem, i)
 
     for ch in range(NCH):
         g_buf[ch, rows(z, SEQ), :] = ffn[:, pl.ds(pl.multiple_of(c * HALF + ch * CW, CW), CW)]
-
-        def z_send(i, carry, ch=ch):
-            z_out(ch, i).start()
-            return carry
-
-        lax.fori_loop(1, NZ, z_send, 0)
+        z_copy(ch, z, 2, za_two.at[ch, 0]).start()
+        z_copy(ch, z, -2, za_two.at[ch, 1]).start()
+        z_copy(ch, z, 1, za_r.at[ch]).start()
+        z_copy(ch, z, -1, za_r.at[ch]).start()
 
     l_sg.wait()
     l_su.wait()
     l_sd.wait()
     hidden = (jax.nn.silu(dot(ffn[...], sg[...])) * dot(ffn[...], su[...])).astype(BF16)
     sh_s[...] = dot(hidden, sd[...]).astype(BF16)
-    sh_copy = remote(sh_s, sh_r, tp_s.at[1], tp_r.at[1], me, 1 - c)
+    sh_copy = to_core(sh_s, sh_r, tp_s.at[2], tp_r.at[2])
     sh_copy.start()
 
-    def meta_wait(i, carry):
-        meta_copy(i, z_peer(i)).wait()
-        return carry
-
-    lax.fori_loop(1, NZ, meta_wait, 0)
+    for ch in range(NCH):
+        for way in range(2):
+            sign = 1 - 2 * way
+            source = z_peer(-2 * sign)
+            z_copy(ch, source, sign, za_two.at[ch, way]).wait_recv()
+            z_copy(ch, source, sign, za_r.at[ch]).start()
+            if ch % 2 == way:
+                z_copy(ch, source, 2 * sign, za_r.at[ch]).start()
+
+    many = meta_r.at[pl.ds(0, NZ - 1)]
+    to_z(many, many, ms_s, ms_r, 1).wait()
     meta = jnp.sum(meta_r[...], axis=0)
     code = meta[0:TOP, :].astype(jnp.int32)
     place = ((code % (2 * NQ)) // 2) * ROWS + (lane // SEQ) * 2 + code % 2
@@ -236,24 +241,23 @@
     whi[...] = high
     wlo[...] = (weight - high.astype(F32)).astype(BF16)
 
-    def q_copy(src, dst, ss, rs, ch, i, at):
-        p = q_peer(i)
-        return remote(src.at[ch, rows(p, ROWS)], dst.at[rows(at, ROWS)], ss.at[ch, i], rs.at[ch, at], z * NQ + p, c)
-
-    for ch in range(NCH):
-
-        def z_wait(i, carry, ch=ch):
-            z_in(ch, i).wait()
+    def q_send(src, dst, ssem, rsem):
+        def send(i, carry):
+            p = q_peer(i)
+            remote(src.at[rows(p, ROWS)], dst.at[rows(q, ROWS)], ssem, rsem, z * NQ + p, c).start()
             return carry
 
-        lax.fori_loop(1, NZ, z_wait, 0)
+        lax.fori_loop(1, NQ, send, 0)
+
+    def q_all(buf, ssem, rsem):
+        part = buf.at[pl.ds(0, (NQ - 1) * ROWS)]
+        return remote(part, part, ssem, rsem, z * NQ + q_peer(1), c)
+
+    for ch in range(NCH):
+        part = g_buf.at[ch, pl.ds(0, 5 * SEQ)]
+        to_z(part, part, za_s.at[ch], za_r.at[ch], 1).wait_recv()
         r_buf[ch] = dot(p_buf[...], g_buf[ch]).astype(BF16)
-
-        def q_send(i, carry, ch=ch):
-            q_copy(r_buf, x_buf.at[c, ch], xa_s, xa_r, ch, i, q).start()
-            return carry
-
-        lax.fori_loop(1, NQ, q_send, 0)
+        q_send(r_buf.at[ch], x_buf.at[c, ch], xa_s.at[ch], xa_r.at[ch])
         x_buf[c, ch, rows(q, ROWS), :] = r_buf[ch, rows(q, ROWS), :]
 
     l_eg.wait()
@@ -262,22 +266,16 @@
     up = jnp.zeros((NQ * ROWS, HID), F32)
     forwards = []
     for ch in range(NCH):
-
-        def q_wait(i, carry, ch=ch):
-            q_copy(r_buf, x_buf.at[c, ch], xa_s, xa_r, ch, i, q_peer(i)).wait()
-            return carry
-
-        lax.fori_loop(1, NQ, q_wait, 0)
-        copy = remote(x_buf.at[c, ch], x_buf.at[c, ch], xf_s.at[ch], xf_r.at[ch], me, 1 - c)
+        q_all(x_buf.at[c, ch], xa_s.at[ch], xa_r.at[ch]).wait_recv()
+        copy = to_core(x_buf.at[c, ch], x_buf.at[c, ch], xf_s.at[ch], xf_r.at[ch])
         copy.start()
         forwards.append(copy)
         depth = rows(c * NCH + ch, CW)
         gate += dot(x_buf[c, ch], eg[0, depth, :])
         up += dot(x_buf[c, ch], eu[0, depth, :])
     for ch in range(NCH):
-        other = remote(x_buf.at[1 - c, ch], x_buf.at[1 - c, ch], xf_s.at[ch], xf_r.at[ch], me, 1 - c)
+        other = to_core(x_buf.at[1 - c, ch], x_buf.at[1 - c, ch], xf_s.at[ch], xf_r.at[ch])
         other.wait_recv()
-        forwards[ch].wait_send()
         depth = rows((1 - c) * NCH + ch, CW)
         gate += dot(x_buf[1 - c, ch], eg[0, depth, :])
         up += dot(x_buf[1 - c, ch], eu[0, depth, :])
@@ -288,66 +286,73 @@
     trades = []
     for ch in range(NCH):
         y_s[ch] = dot(hid_v[...], ed[1 - c, :, ch * CW : (ch + 1) * CW]).astype(BF16)
-        copy = remote(y_s.at[ch], y_r.at[ch], yx_s.at[ch], yx_r.at[ch], me, 1 - c)
+        copy = to_core(y_s.at[ch], y_r.at[ch], yx_s.at[ch], yx_r.at[ch])
         copy.start()
         trades.append(copy)
     for ch in range(NCH):
         own = dot(hid_v[...], ed[c, :, ch * CW : (ch + 1) * CW]).astype(BF16).astype(F32)
         trades[ch].wait()
         o_buf[ch] = (own + y_r[ch].astype(F32)).astype(BF16)
-
-        def back_send(i, carry, ch=ch):
-            q_copy(o_buf, b_buf.at[ch], xb_s, xb_r, ch, i, q).start()
-            return carry
-
-        lax.fori_loop(1, NQ, back_send, 0)
+        q_send(o_buf.at[ch], b_buf.at[ch], xb_s.at[ch], xb_r.at[ch])
         b_buf[ch, rows(q, ROWS), :] = o_buf[ch, rows(q, ROWS), :]
 
-    def sum_copy(ch, i, at):
-        p = z_peer(i)
-        return remote(
-            t_buf.at[ch, rows(p, SEQ)], v_buf.at[ch, rows(at, SEQ)], zb_s.at[ch, i], zb_r.at[ch, at], p * NQ + q, c
-        )
-
-    for ch in range(NCH):
-
-        def back_wait(i, carry, ch=ch):
-            q_copy(o_buf, b_buf.at[ch], xb_s, xb_r, ch, i, q_peer(i)).wait()
-            return carry
-
-        lax.fori_loop(1, NQ, back_wait, 0)
+    def weighted(ch):
+        q_all(b_buf.at[ch], xb_s.at[ch], xb_r.at[ch]).wait_recv()
         t_buf[ch] = (dot(whi[...], b_buf[ch]) + dot(wlo[...], b_buf[ch])).astype(BF16)
-
-        def sum_send(i, carry, ch=ch):
-            sum_copy(ch, i, z).start()
-            return carry
-
-        lax.fori_loop(1, NZ, sum_send, 0)
-        v_buf[ch, rows(z, SEQ), :] = t_buf[ch, rows(z, SEQ), :]
+        for way in range(2):
+            sign = 1 - 2 * way
+            two = zb_two.at[ch, way]
+            if ch % 2 == way:
+                to_z(t_buf.at[ch, rows(z_peer(4), SEQ)], rl_buf.at[ch, way, 1], zb_s.at[ch], two, -2 * sign).start()
+            to_z(t_buf.at[ch, rows(z_peer(-3 * sign), SEQ)], rl_buf.at[ch, way, 0], zb_s.at[ch], two, -sign).start()
+        for way in range(2):
+            sign = 1 - 2 * way
+            to_z(t_buf.at[ch, rows(z_peer(-sign), SEQ)], v_buf.at[ch, way], zb_s.at[ch], zb_r.at[ch], -sign).start()
+
+    def relayed(ch):
+        for way in range(2):
+            sign = 1 - 2 * way
+            many = rl_buf.at[ch, way, pl.ds(0, 2 if ch % 2 == way else 1)]
+            to_z(many, many, zb_s.at[ch], zb_two.at[ch, way], 1).wait_recv()
+            total = t_buf[ch, rows(z_peer(-2 * sign), SEQ), :].astype(F32) + rl_buf[ch, way, 0].astype(F32)
+            if ch % 2 == way:
+                total += rl_buf[ch, way, 1].astype(F32)
+            c_buf[ch, way] = total.astype(BF16)
+            to_z(c_buf.at[ch, way], v_buf.at[ch, 2 + way], zb_s.at[ch], zb_r.at[ch], -2 * sign).start()
+
+    for ch in range(NCH):
+        weighted(ch)
+        if ch >= 2:
+            relayed(ch - 2)
+    for ch in range(NCH - 2, NCH):
+        relayed(ch)
 
     sh_copy.wait()
     shared = sh_s[...].astype(F32) + sh_r[...].astype(F32)
     pairs = []
     for ch in range(NCH):
-
-        def sum_wait(i, carry, ch=ch):
-            sum_copy(ch, i, z_peer(i)).wait()
-            return carry
-
-        lax.fori_loop(1, NZ, sum_wait, 0)
-        total = v_buf[ch, 0:SEQ, :].astype(F32)
-        for s in range(1, NZ):
-            total += v_buf[ch, s * SEQ : (s + 1) * SEQ, :].astype(F32)
+        to_z(v_buf.at[ch], v_buf.at[ch], zb_s.at[ch], zb_r.at[ch], 1).wait_recv()
+        total = t_buf[ch, rows(z, SEQ), :].astype(F32)
+        for s in range(4):
+            total += v_buf[ch, s].astype(F32)
         rt_buf[c, ch] = total.astype(BF16)
-        copy = remote(rt_buf.at[c, ch], rt_buf.at[c, ch], rt_s.at[ch], rt_r.at[ch], me, 1 - c)
+        copy = to_core(rt_buf.at[c, ch], rt_buf.at[c, ch], rt_s.at[ch], rt_r.at[ch])
         copy.start()
         pairs.append(copy)
     for ch in range(NCH):
-        remote(rt_buf.at[1 - c, ch], rt_buf.at[1 - c, ch], rt_s.at[ch], rt_r.at[ch], me, 1 - c).wait_recv()
-        pairs[ch].wait_send()
+        to_core(rt_buf.at[1 - c, ch], rt_buf.at[1 - c, ch], rt_s.at[ch], rt_r.at[ch]).wait_recv()
     routed = jnp.concatenate([rt_buf[h, ch] for h in range(2) for ch in range(NCH)], axis=1)
     last = scaled(routed.astype(F32) + shared, gains[3])
     out_v[...] = (middle_v[...].astype(F32) + last).astype(BF16)
+
+    for ch in range(NCH):
+        for buf, sem in ((g_buf, za_s), (t_buf, zb_s)):
+            part = buf.at[ch, pl.ds(0, 7 * SEQ)]
+            to_z(part, part, sem.at[ch], za_r.at[ch], 1).wait_send()
+        q_all(r_buf.at[ch], xa_s.at[ch], xa_r.at[ch]).wait_send()
+        q_all(o_buf.at[ch], xb_s.at[ch], xb_r.at[ch]).wait_send()
+        forwards[ch].wait_send()
+        pairs[ch].wait_send()
 
 
 def store(*refs):
@@ -378,15 +383,17 @@
         vmem(TOP, SEQ, dtype=jnp.int32), vmem(TOP, SEQ, dtype=F32),
         vmem(1, D, HID), vmem(1, D, HID), vmem(2, HID, HALF), vmem(D, HID), vmem(D, HID), vmem(HID, D),
         vmem(SEQ, D), vmem(SEQ, D),
-        vmem(SEQ, D), vmem(SEQ, D), vmem(2 * TOP, NZ * SEQ, dtype=F32), vmem(NZ, 2 * TOP, NZ * SEQ, dtype=F32),
+        vmem(2, SEQ, HALF), vmem(2, SEQ, HALF), vmem(2 * TOP, NZ * SEQ, dtype=F32), vmem(NZ, 2 * TOP, NZ * SEQ, dtype=F32),
         vmem(SEQ, D), vmem(SEQ, D),
         vmem(NCH, NZ * SEQ, CW), vmem(NCH, NQ * ROWS, CW), vmem(2, NCH, NQ * ROWS, CW),
         vmem(NQ * ROWS, NZ * SEQ), vmem(NZ * SEQ, NQ * ROWS), vmem(NZ * SEQ, NQ * ROWS), vmem(NQ * ROWS, HID),
         vmem(NCH, NQ * ROWS, CW), vmem(NCH, NQ * ROWS, CW), vmem(NCH, NQ * ROWS, CW), vmem(NCH, NQ * ROWS, CW),
-        vmem(NCH, NZ * SEQ, CW), vmem(NCH, NZ * SEQ, CW), vmem(2, NCH, SEQ, CW),
+        vmem(NCH, NZ * SEQ, CW), vmem(NCH, 2, 2, SEQ, CW), vmem(NCH, 2, SEQ, CW), vmem(NCH, 4, SEQ, CW),
+        vmem(2, NCH, SEQ, CW),
         dma(29),
-        dma(2), dma(2), dma(NZ), dma(NZ), dma(NCH, NZ), dma(NCH, NZ), dma(NCH, NQ), dma(NCH, NQ), dma(NCH), dma(NCH),
-        dma(NCH), dma(NCH), dma(NCH, NQ), dma(NCH, NQ), dma(NCH, NZ), dma(NCH, NZ), dma(NCH), dma(NCH),
+        dma(3), dma(3), pltpu.SemaphoreType.DMA, pltpu.SemaphoreType.DMA, dma(NCH), dma(NCH, 2), dma(NCH), dma(NCH),
+        dma(NCH), dma(NCH), dma(NCH), dma(NCH), dma(NCH), dma(NCH), dma(NCH), dma(NCH), dma(NCH, 2), dma(NCH), dma(NCH),
+        dma(NCH),
     ]
     vm = pl.BlockSpec(memory_space=pltpu.VMEM)
     results = pl.pallas_call(

time: 61.2 us -> 54.2 us (0.89)
  Pallas kernels: 60.5 us -> 53.5 us
    pallas_call x1, Pallas kernels: 59.7 us -> 52.8 us  [on_device(): pl.pallas_call(kernel, out_shape=(pltpu.VMEM((SEQ, D), BF16), pltpu.VMEM(...]
where the time goes in v3:
time: 54.2 us; the launch traced here: 54.1 us
  Pallas kernels  53.5 us (99%)
  between operations  0.65 us (1%)
    pallas_call x1, Pallas kernels, on_device(): pl.pallas_call(kernel, out_shape=(pltpu.VMEM((SEQ, D), BF16), pltpu.VMEM(...  52.8 us

profile of v3, /device:TPU:1, one launch (start us, length us, event | category | flops | bytes accessed | tf_op | source)
XLA Modules:
  0.0 54.1 jit_solution(3446693488511345015)
XLA Ops:
  0.6 52.8 %layer.1 = (bf16[32,2048]{1,0:T(8,128)(2,1)S(1)}, f32[32,512]{1,0:T(8,128)S(1)}, bf16[3,32,512]{2,1,0:T(8,128)(2,1)S(1)}) custom-call(bf16[32,2048]{1,0:T(8,128)(2,1)} %tok_h.1, f32[32,512]{1,0:T(8,128)} %lru_h.1, bf16[3,32,512]{2,1,0:T(8,128)(2,1)} %bitcast.11, bf16[4,512]{1,0:T(4,128)(2,1)} %taps_h.1, f32[1,2048]{1,0:T(1,128)} %bitcast.12, ...), custom_call_target="tpu_custom_call" | custom-call | tf_op jit(solution)/shard_map/layer/pallas_call | solution.py:399
  53.4 0.7 %store.1 = (bf16[32,2048]{1,0:T(8,128)(2,1)}, f32[32,512]{1,0:T(8,128)}, bf16[3,32,512]{2,1,0:T(8,128)(2,1)}) custom-call(bf16[32,2048]{1,0:T(8,128)(2,1)S(1)} %get-tuple-element.9.refs_0_, f32[32,512]{1,0:T(8,128)S(1)} %get-tuple-element.10.refs_1_, bf16[3,32,512]{2,1,0:T(8,128)(2,1)S(1)} %get-tuple-element.11.refs_2_), custom_call_target="tpu_custom_call" | custom-call | tf_op jit(solution)/shard_map/store/pallas_call | solution.py:416

commit v4 on v3

--- a/solution.py
+++ b/solution.py
@@ -17,8 +17,10 @@
 TOP = 4
 D = 2048
 HALF = D // 2
-NCH = 4
-CW = HALF // NCH
+WIDTHS = (256, 384, 256, 128)
+NCH = len(WIDTHS)
+STARTS = tuple(sum(WIDTHS[:i]) for i in range(NCH))
+FAR = (10, 11, 9, 14, 6, 15, 5, 13, 7, 2, 8, 3, 1, 12, 4)
 LC = 512
 HID = 256
 ROWS = NZ * 2
@@ -55,26 +57,15 @@
     def z_peer(i):
         return lax.rem(z + (i + NZ), NZ)
 
+    y_peer = [lax.rem(y + i, 4) * 4 for i in range(4)]
+    x_peer = [lax.rem(x + i, 4) for i in range(4)]
+
     def q_peer(i):
-        return lax.rem(y + i // 4, 4) * 4 + lax.rem(x + i % 4, 4)
+        return y_peer[i // 4] + x_peer[i % 4]
 
     def rows(i, n):
         return pl.ds(pl.multiple_of(i * n, n), n)
 
-    barrier = pltpu.get_barrier_semaphore()
-    pl.semaphore_signal(barrier, inc=1, device_id=(me, 1 - c), device_id_type=MESH)
-
-    def greet_z(i, carry):
-        pl.semaphore_signal(barrier, inc=1, device_id=(z_peer(i) * NQ + q, c), device_id_type=MESH)
-        return carry
-
-    def greet_q(i, carry):
-        pl.semaphore_signal(barrier, inc=1, device_id=(z * NQ + q_peer(i), c), device_id_type=MESH)
-        return carry
-
-    lax.fori_loop(1, NZ, greet_z, 0)
-    lax.fori_loop(1, NQ, greet_q, 0)
-
     def load(k, src, dst):
         copy = pltpu.make_async_copy(src, dst, lsem.at[k])
         copy.start()
@@ -82,22 +73,33 @@
 
     step = D // NPIECE
     l_tok = load(0, tok_h, tok)
-    l_gains = [load(1 + i, h, gains.at[i]) for i, h in enumerate((gain0_h, gain1_h, gain2_h, gain3_h))]
+    l_gains = [load(1, gain0_h, gains.at[0])]
     l_wi = [load(5 + i, wi_h.at[pl.ds(i * step, step)], wi.at[pl.ds(i * step, step)]) for i in range(NPIECE)]
     l_win = load(9, win_h, win)
     l_taps = load(10, taps_h, taps)
     l_ga = load(11, ga_h, ga)
     l_gx = load(12, gx_h, gx)
+    l_decay = load(19, decay_h, decay)
+    l_lru = load(20, lru_h, lru)
+    l_wb = [load(15 + i, wb_h.at[pl.ds(i * step, step)], wb.at[pl.ds(i * step, step)]) for i in range(NPIECE)]
+    l_wm = [load(21 + i, wm_h.at[:, pl.ds(i * HALF, HALF)], wm.at[i]) for i in range(2)]
     l_routes = load(13, routes_h, routes)
     l_rweight = load(14, rweight_h, rweight)
-    l_wb = [load(15 + i, wb_h.at[pl.ds(i * step, step)], wb.at[pl.ds(i * step, step)]) for i in range(NPIECE)]
-    l_decay = load(19, decay_h, decay)
-    l_lru = load(20, lru_h, lru)
-    l_wm = load(21, wm_h, wm)
+    l_gains += [load(1 + i, h, gains.at[i]) for i, h in ((1, gain1_h), (2, gain2_h), (3, gain3_h))]
+
+    barrier = pltpu.get_barrier_semaphore()
+    pl.semaphore_signal(barrier, inc=1, device_id=(me, 1 - c), device_id_type=MESH)
+
+    def greet_z(i, carry):
+        pl.semaphore_signal(barrier, inc=1, device_id=(z_peer(i) * NQ + q, c), device_id_type=MESH)
+        return carry
+
+    lax.fori_loop(1, NZ, greet_z, 0)
+    for i in FAR:
+        pl.semaphore_signal(barrier, inc=1, device_id=(z * NQ + q_peer(i), c), device_id_type=MESH)
 
     l_tok.wait()
-    for copy in l_gains:
-        copy.wait()
+    l_gains[0].wait()
     normed = scaled(tok[...].astype(F32), gains[0]).astype(BF16)
     inflow = jnp.zeros((SEQ, LC), F32)
     for i in range(NPIECE):
@@ -129,16 +131,16 @@
         l_wb[i].wait()
         branch += dot(normed[:, i * step : (i + 1) * step], wb[i * step : (i + 1) * step, :])
     gated = (state * jax.nn.gelu(branch)).astype(BF16)
-    l_wm.wait()
     for i in range(2):
-        mix_s[i] = dot(gated, wm[:, i * HALF : (i + 1) * HALF]).astype(BF16)
-
-    l_sg = load(22, sg_h, sg)
-    l_su = load(23, su_h, su)
-    l_sd = load(24, sd_h, sd)
-    l_eg = load(25, eg_h, eg)
-    l_eu = load(26, eu_h, eu)
-    l_ed = [load(27 + i, ed_h.at[:, pl.ds(i * HALF, HALF)], ed.at[i]) for i in range(2)]
+        l_wm[i].wait()
+        mix_s[i] = dot(gated, wm[i]).astype(BF16)
+
+    l_sg = load(23, sg_h, sg)
+    l_su = load(24, su_h, su)
+    l_sd = load(25, sd_h, sd)
+    l_eg = load(26, eg_h, eg)
+    l_eu = load(27, eu_h, eu)
+    l_ed = [load(28 + i, ed_h.at[:, pl.ds(i * HALF, HALF)], ed.at[i]) for i in range(2)]
 
     pl.semaphore_wait(barrier, 1 + (NZ - 1) + (NQ - 1))
 
@@ -185,6 +187,8 @@
 
     lax.fori_loop(1, NZ, meta_send, 0)
 
+    for copy in l_gains[1:]:
+        copy.wait()
     mixed = []
     for i in range(2):
         mix_copies[i].wait()
@@ -195,15 +199,28 @@
     ffn[...] = scaled(middle.astype(F32), gains[2]).astype(BF16)
 
     def z_copy(ch, source, i, rsem):
-        block = g_buf.at[ch, rows(source, SEQ)]
+        block = g_buf[ch].at[rows(source, SEQ)]
         return to_z(block, block, za_s.at[ch], rsem, i)
 
-    for ch in range(NCH):
-        g_buf[ch, rows(z, SEQ), :] = ffn[:, pl.ds(pl.multiple_of(c * HALF + ch * CW, CW), CW)]
+    def direct(ch):
+        columns = pl.ds(pl.multiple_of(c * HALF + STARTS[ch], 128), WIDTHS[ch])
+        g_buf[ch][rows(z, SEQ), :] = ffn[:, columns]
         z_copy(ch, z, 2, za_two.at[ch, 0]).start()
         z_copy(ch, z, -2, za_two.at[ch, 1]).start()
         z_copy(ch, z, 1, za_r.at[ch]).start()
         z_copy(ch, z, -1, za_r.at[ch]).start()
+
+    def relay(ch):
+        for way in range(2):
+            sign = 1 - 2 * way
+            source = z_peer(-2 * sign)
+            z_copy(ch, source, sign, za_two.at[ch, way]).wait_recv()
+            if ch % 2 == way:
+                z_copy(ch, source, 2 * sign, za_r.at[ch]).start()
+            z_copy(ch, source, sign, za_r.at[ch]).start()
+
+    for ch in range(NCH - 1):
+        direct(ch)
 
     l_sg.wait()
     l_su.wait()
@@ -213,14 +230,9 @@
     sh_copy = to_core(sh_s, sh_r, tp_s.at[2], tp_r.at[2])
     sh_copy.start()
 
-    for ch in range(NCH):
-        for way in range(2):
-            sign = 1 - 2 * way
-            source = z_peer(-2 * sign)
-            z_copy(ch, source, sign, za_two.at[ch, way]).wait_recv()
-            z_copy(ch, source, sign, za_r.at[ch]).start()
-            if ch % 2 == way:
-                z_copy(ch, source, 2 * sign, za_r.at[ch]).start()
+    relay(0)
+    direct(NCH - 1)
+    relay(1)
 
     many = meta_r.at[pl.ds(0, NZ - 1)]
     to_z(many, many, ms_s, ms_r, 1).wait()
@@ -242,23 +254,27 @@
     wlo[...] = (weight - high.astype(F32)).astype(BF16)
 
     def q_send(src, dst, ssem, rsem):
-        def send(i, carry):
+        for i in FAR:
             p = q_peer(i)
             remote(src.at[rows(p, ROWS)], dst.at[rows(q, ROWS)], ssem, rsem, z * NQ + p, c).start()
-            return carry
-
-        lax.fori_loop(1, NQ, send, 0)
 
     def q_all(buf, ssem, rsem):
         part = buf.at[pl.ds(0, (NQ - 1) * ROWS)]
         return remote(part, part, ssem, rsem, z * NQ + q_peer(1), c)
 
-    for ch in range(NCH):
-        part = g_buf.at[ch, pl.ds(0, 5 * SEQ)]
+    def picked(ch):
+        part = g_buf[ch].at[pl.ds(0, 5 * SEQ)]
         to_z(part, part, za_s.at[ch], za_r.at[ch], 1).wait_recv()
-        r_buf[ch] = dot(p_buf[...], g_buf[ch]).astype(BF16)
-        q_send(r_buf.at[ch], x_buf.at[c, ch], xa_s.at[ch], xa_r.at[ch])
-        x_buf[c, ch, rows(q, ROWS), :] = r_buf[ch, rows(q, ROWS), :]
+        r_buf[ch][...] = dot(p_buf[...], g_buf[ch][...]).astype(BF16)
+        q_send(r_buf[ch], x_buf[ch].at[c], xa_s.at[ch], xa_r.at[ch])
+        x_buf[ch][c, rows(q, ROWS), :] = r_buf[ch][rows(q, ROWS), :]
+
+    relay(2)
+    picked(0)
+    relay(3)
+    picked(1)
+    picked(2)
+    picked(3)
 
     l_eg.wait()
     l_eu.wait()
@@ -266,93 +282,114 @@
     up = jnp.zeros((NQ * ROWS, HID), F32)
     forwards = []
     for ch in range(NCH):
-        q_all(x_buf.at[c, ch], xa_s.at[ch], xa_r.at[ch]).wait_recv()
-        copy = to_core(x_buf.at[c, ch], x_buf.at[c, ch], xf_s.at[ch], xf_r.at[ch])
+        q_all(x_buf[ch].at[c], xa_s.at[ch], xa_r.at[ch]).wait_recv()
+        copy = to_core(x_buf[ch].at[c], x_buf[ch].at[c], xf_s.at[ch], xf_r.at[ch])
         copy.start()
         forwards.append(copy)
-        depth = rows(c * NCH + ch, CW)
-        gate += dot(x_buf[c, ch], eg[0, depth, :])
-        up += dot(x_buf[c, ch], eu[0, depth, :])
+        depth = pl.ds(pl.multiple_of(c * HALF + STARTS[ch], 128), WIDTHS[ch])
+        gate += dot(x_buf[ch][c], eg[0, depth, :])
+        up += dot(x_buf[ch][c], eu[0, depth, :])
     for ch in range(NCH):
-        other = to_core(x_buf.at[1 - c, ch], x_buf.at[1 - c, ch], xf_s.at[ch], xf_r.at[ch])
+        other = to_core(x_buf[ch].at[1 - c], x_buf[ch].at[1 - c], xf_s.at[ch], xf_r.at[ch])
         other.wait_recv()
-        depth = rows((1 - c) * NCH + ch, CW)
-        gate += dot(x_buf[1 - c, ch], eg[0, depth, :])
-        up += dot(x_buf[1 - c, ch], eu[0, depth, :])
+        depth = pl.ds(pl.multiple_of((1 - c) * HALF + STARTS[ch], 128), WIDTHS[ch])
+        gate += dot(x_buf[ch][1 - c], eg[0, depth, :])
+        up += dot(x_buf[ch][1 - c], eu[0, depth, :])
     hid_v[...] = (jax.nn.silu(gate) * up).astype(BF16)
 
     for copy in l_ed:
         copy.wait()
     trades = []
-    for ch in range(NCH):
-        y_s[ch] = dot(hid_v[...], ed[1 - c, :, ch * CW : (ch + 1) * CW]).astype(BF16)
-        copy = to_core(y_s.at[ch], y_r.at[ch], yx_s.at[ch], yx_r.at[ch])
+
+    def down(core, ch):
+        return dot(hid_v[...], ed[core, :, STARTS[ch] : STARTS[ch] + WIDTHS[ch]]).astype(BF16)
+
+    def trade(ch):
+        y_s[ch][...] = down(1 - c, ch)
+        copy = to_core(y_s[ch], y_r[ch], yx_s.at[ch], yx_r.at[ch])
         copy.start()
         trades.append(copy)
-    for ch in range(NCH):
-        own = dot(hid_v[...], ed[c, :, ch * CW : (ch + 1) * CW]).astype(BF16).astype(F32)
+
+    def back(ch):
+        own = down(c, ch).astype(F32)
         trades[ch].wait()
-        o_buf[ch] = (own + y_r[ch].astype(F32)).astype(BF16)
-        q_send(o_buf.at[ch], b_buf.at[ch], xb_s.at[ch], xb_r.at[ch])
-        b_buf[ch, rows(q, ROWS), :] = o_buf[ch, rows(q, ROWS), :]
+        o_buf[ch][...] = (own + y_r[ch][...].astype(F32)).astype(BF16)
+        q_send(o_buf[ch], b_buf[ch], xb_s.at[ch], xb_r.at[ch])
+        b_buf[ch][rows(q, ROWS), :] = o_buf[ch][rows(q, ROWS), :]
+
+    trade(0)
+    trade(1)
+    back(0)
+    trade(2)
+    back(1)
+    trade(3)
+    back(2)
+    back(3)
 
     def weighted(ch):
-        q_all(b_buf.at[ch], xb_s.at[ch], xb_r.at[ch]).wait_recv()
-        t_buf[ch] = (dot(whi[...], b_buf[ch]) + dot(wlo[...], b_buf[ch])).astype(BF16)
+        q_all(b_buf[ch], xb_s.at[ch], xb_r.at[ch]).wait_recv()
+        t_buf[ch][...] = (dot(whi[...], b_buf[ch][...]) + dot(wlo[...], b_buf[ch][...])).astype(BF16)
+        sem = zb_s.at[ch]
+        if ch == NCH - 1:
+            for slot, i in enumerate((4, 3, -3, 2, -2, 1, -1)):
+                to_z(t_buf[ch].at[rows(z_peer(i), SEQ)], v_buf[ch].at[slot], sem, zb_r.at[ch], i).start()
+            return
         for way in range(2):
             sign = 1 - 2 * way
             two = zb_two.at[ch, way]
             if ch % 2 == way:
-                to_z(t_buf.at[ch, rows(z_peer(4), SEQ)], rl_buf.at[ch, way, 1], zb_s.at[ch], two, -2 * sign).start()
-            to_z(t_buf.at[ch, rows(z_peer(-3 * sign), SEQ)], rl_buf.at[ch, way, 0], zb_s.at[ch], two, -sign).start()
+                to_z(t_buf[ch].at[rows(z_peer(4), SEQ)], rl_buf[ch].at[way, 1], sem, two, -2 * sign).start()
+            to_z(t_buf[ch].at[rows(z_peer(-3 * sign), SEQ)], rl_buf[ch].at[way, 0], sem, two, -sign).start()
         for way in range(2):
             sign = 1 - 2 * way
-            to_z(t_buf.at[ch, rows(z_peer(-sign), SEQ)], v_buf.at[ch, way], zb_s.at[ch], zb_r.at[ch], -sign).start()
+            to_z(t_buf[ch].at[rows(z_peer(-sign), SEQ)], v_buf[ch].at[way], sem, zb_r.at[ch], -sign).start()
 
     def relayed(ch):
         for way in range(2):
             sign = 1 - 2 * way
-            many = rl_buf.at[ch, way, pl.ds(0, 2 if ch % 2 == way else 1)]
+            many = rl_buf[ch].at[way, pl.ds(0, 2 if ch % 2 == way else 1)]
             to_z(many, many, zb_s.at[ch], zb_two.at[ch, way], 1).wait_recv()
-            total = t_buf[ch, rows(z_peer(-2 * sign), SEQ), :].astype(F32) + rl_buf[ch, way, 0].astype(F32)
+            total = t_buf[ch][rows(z_peer(-2 * sign), SEQ), :].astype(F32) + rl_buf[ch][way, 0].astype(F32)
             if ch % 2 == way:
-                total += rl_buf[ch, way, 1].astype(F32)
-            c_buf[ch, way] = total.astype(BF16)
-            to_z(c_buf.at[ch, way], v_buf.at[ch, 2 + way], zb_s.at[ch], zb_r.at[ch], -2 * sign).start()
-
-    for ch in range(NCH):
-        weighted(ch)
-        if ch >= 2:
-            relayed(ch - 2)
-    for ch in range(NCH - 2, NCH):
-        relayed(ch)
+                total += rl_buf[ch][way, 1].astype(F32)
+            c_buf[ch][way] = total.astype(BF16)
+            to_z(c_buf[ch].at[way], v_buf[ch].at[2 + way], zb_s.at[ch], zb_r.at[ch], -2 * sign).start()
+
+    weighted(0)
+    weighted(1)
+    relayed(0)
+    weighted(2)
+    relayed(1)
+    weighted(3)
+    relayed(2)
 
     sh_copy.wait()
     shared = sh_s[...].astype(F32) + sh_r[...].astype(F32)
     pairs = []
     for ch in range(NCH):
-        to_z(v_buf.at[ch], v_buf.at[ch], zb_s.at[ch], zb_r.at[ch], 1).wait_recv()
-        total = t_buf[ch, rows(z, SEQ), :].astype(F32)
-        for s in range(4):
-            total += v_buf[ch, s].astype(F32)
-        rt_buf[c, ch] = total.astype(BF16)
-        copy = to_core(rt_buf.at[c, ch], rt_buf.at[c, ch], rt_s.at[ch], rt_r.at[ch])
+        to_z(v_buf[ch], v_buf[ch], zb_s.at[ch], zb_r.at[ch], 1).wait_recv()
+        total = t_buf[ch][rows(z, SEQ), :].astype(F32)
+        for s in range(7 if ch == NCH - 1 else 4):
+            total += v_buf[ch][s].astype(F32)
+        rt_buf[ch][c] = total.astype(BF16)
+        copy = to_core(rt_buf[ch].at[c], rt_buf[ch].at[c], rt_s.at[ch], rt_r.at[ch])
         copy.start()
         pairs.append(copy)
+
     for ch in range(NCH):
-        to_core(rt_buf.at[1 - c, ch], rt_buf.at[1 - c, ch], rt_s.at[ch], rt_r.at[ch]).wait_recv()
-    routed = jnp.concatenate([rt_buf[h, ch] for h in range(2) for ch in range(NCH)], axis=1)
+        for buf, sem in ((g_buf, za_s), (t_buf, zb_s)):
+            part = buf[ch].at[pl.ds(0, 7 * SEQ)]
+            to_z(part, part, sem.at[ch], za_r.at[ch], 1).wait_send()
+        q_all(r_buf[ch], xa_s.at[ch], xa_r.at[ch]).wait_send()
+        q_all(o_buf[ch], xb_s.at[ch], xb_r.at[ch]).wait_send()
+        forwards[ch].wait_send()
+    for ch in range(NCH):
+        to_core(rt_buf[ch].at[1 - c], rt_buf[ch].at[1 - c], rt_s.at[ch], rt_r.at[ch]).wait_recv()
+    routed = jnp.concatenate([rt_buf[ch][h] for h in range(2) for ch in range(NCH)], axis=1)
     last = scaled(routed.astype(F32) + shared, gains[3])
     out_v[...] = (middle_v[...].astype(F32) + last).astype(BF16)
-
-    for ch in range(NCH):
-        for buf, sem in ((g_buf, za_s), (t_buf, zb_s)):
-            part = buf.at[ch, pl.ds(0, 7 * SEQ)]
-            to_z(part, part, sem.at[ch], za_r.at[ch], 1).wait_send()
-        q_all(r_buf.at[ch], xa_s.at[ch], xa_r.at[ch]).wait_send()
-        q_all(o_buf.at[ch], xb_s.at[ch], xb_r.at[ch]).wait_send()
-        forwards[ch].wait_send()
-        pairs[ch].wait_send()
+    for copy in pairs:
+        copy.wait_send()
 
 
 def store(*refs):
@@ -374,23 +411,26 @@
     def vmem(*shape, dtype=BF16):
         return pltpu.VMEM(shape, dtype)
 
+    def chunks(*shape):
+        return [vmem(*shape, width) for width in WIDTHS]
+
     def dma(*shape):
         return pltpu.SemaphoreType.DMA(shape)
 
     scratch = [
         vmem(SEQ, D), vmem(SEQ, LC, dtype=F32), vmem(3, SEQ, LC), vmem(4, LC), vmem(4, 1, D, dtype=F32),
-        vmem(1, LC, dtype=F32), vmem(D, LC), vmem(D, LC), vmem(4, 128, 128), vmem(4, 128, 128), vmem(LC, D),
+        vmem(1, LC, dtype=F32), vmem(D, LC), vmem(D, LC), vmem(4, 128, 128), vmem(4, 128, 128), vmem(2, LC, HALF),
         vmem(TOP, SEQ, dtype=jnp.int32), vmem(TOP, SEQ, dtype=F32),
         vmem(1, D, HID), vmem(1, D, HID), vmem(2, HID, HALF), vmem(D, HID), vmem(D, HID), vmem(HID, D),
         vmem(SEQ, D), vmem(SEQ, D),
         vmem(2, SEQ, HALF), vmem(2, SEQ, HALF), vmem(2 * TOP, NZ * SEQ, dtype=F32), vmem(NZ, 2 * TOP, NZ * SEQ, dtype=F32),
         vmem(SEQ, D), vmem(SEQ, D),
-        vmem(NCH, NZ * SEQ, CW), vmem(NCH, NQ * ROWS, CW), vmem(2, NCH, NQ * ROWS, CW),
+        chunks(NZ * SEQ), chunks(NQ * ROWS), chunks(2, NQ * ROWS),
         vmem(NQ * ROWS, NZ * SEQ), vmem(NZ * SEQ, NQ * ROWS), vmem(NZ * SEQ, NQ * ROWS), vmem(NQ * ROWS, HID),
-        vmem(NCH, NQ * ROWS, CW), vmem(NCH, NQ * ROWS, CW), vmem(NCH, NQ * ROWS, CW), vmem(NCH, NQ * ROWS, CW),
-        vmem(NCH, NZ * SEQ, CW), vmem(NCH, 2, 2, SEQ, CW), vmem(NCH, 2, SEQ, CW), vmem(NCH, 4, SEQ, CW),
-        vmem(2, NCH, SEQ, CW),
-        dma(29),
+        chunks(NQ * ROWS), chunks(NQ * ROWS), chunks(NQ * ROWS), chunks(NQ * ROWS),
+        chunks(NZ * SEQ), chunks(2, 2, SEQ), chunks(2, SEQ),
+        [vmem(7 if ch == NCH - 1 else 4, SEQ, WIDTHS[ch]) for ch in range(NCH)], chunks(2, SEQ),
+        dma(30),
         dma(3), dma(3), pltpu.SemaphoreType.DMA, pltpu.SemaphoreType.DMA, dma(NCH), dma(NCH, 2), dma(NCH), dma(NCH),
         dma(NCH), dma(NCH), dma(NCH), dma(NCH), dma(NCH), dma(NCH), dma(NCH), dma(NCH), dma(NCH, 2), dma(NCH), dma(NCH),
         dma(NCH),

time: 54.2 us -> 53.9 us (level)
  no operation moved by 1% of the time
where the time goes in v4:
time: 53.9 us; the launch traced here: 53.8 us
  Pallas kernels  53.2 us (99%)
  between operations  0.65 us (1%)
    pallas_call x1, Pallas kernels, on_device(): pl.pallas_call(kernel, out_shape=(pltpu.VMEM((SEQ, D), BF16), pltpu.VMEM(...  52.4 us

profile of v4, /device:TPU:1, one launch (start us, length us, event | category | flops | bytes accessed | tf_op | source)
XLA Modules:
  0.0 53.8 jit_solution(16863369864300060803)
XLA Ops:
  0.6 52.4 %layer.1 = (bf16[32,2048]{1,0:T(8,128)(2,1)S(1)}, f32[32,512]{1,0:T(8,128)S(1)}, bf16[3,32,512]{2,1,0:T(8,128)(2,1)S(1)}) custom-call(bf16[32,2048]{1,0:T(8,128)(2,1)} %tok_h.1, f32[32,512]{1,0:T(8,128)} %lru_h.1, bf16[3,32,512]{2,1,0:T(8,128)(2,1)} %bitcast.11, bf16[4,512]{1,0:T(4,128)(2,1)} %taps_h.1, f32[1,2048]{1,0:T(1,128)} %bitcast.12, ...), custom_call_target="tpu_custom_call" | custom-call | tf_op jit(solution)/shard_map/layer/pallas_call | solution.py:439
  53.1 0.7 %store.1 = (bf16[32,2048]{1,0:T(8,128)(2,1)}, f32[32,512]{1,0:T(8,128)}, bf16[3,32,512]{2,1,0:T(8,128)(2,1)}) custom-call(bf16[32,2048]{1,0:T(8,128)(2,1)S(1)} %get-tuple-element.9.refs_0_, f32[32,512]{1,0:T(8,128)S(1)} %get-tuple-element.10.refs_1_, bf16[3,32,512]{2,1,0:T(8,128)(2,1)S(1)} %get-tuple-element.11.refs_2_), custom_call_target="tpu_custom_call" | custom-call | tf_op jit(solution)/shard_map/store/pallas_call | solution.py:456

commit v5 on v4

v5 whole, which is shorter than its diff:
```python
import functools

import jax
import jax.numpy as jnp
from jax import lax
from jax.experimental import pallas as pl
from jax.experimental.pallas import tpu as pltpu
from jax.sharding import PartitionSpec as P

MESH = pl.DeviceIdType.MESH
F32 = jnp.float32
BF16 = jnp.bfloat16

NZ = 8
NQ = 16
SEQ = 32
TOP = 4
D = 2048
HALF = D // 2
WIDTHS = (256, 512, 256)
NCH = len(WIDTHS)
STARTS = tuple(sum(WIDTHS[:i]) for i in range(NCH))
FAR = (10, 11, 9, 14, 6, 15, 5, 13, 7, 2, 8, 3, 1, 12, 4)
LC = 512
HID = 256
ROWS = NZ * 2
NLOAD = 20
PLUS = (0, 1, 0)
PIECES = ((0, 768), (768, 768), (1536, 512))


def scaled(value, gain):
    return value * lax.rsqrt(jnp.mean(value * value, axis=-1, keepdims=True) + 1e-06) * gain


def dot(a, b):
    return jnp.dot(a, b, preferred_element_type=F32)


def kernel(
    tok_h, lru_h, win_h, taps_h, gain0_h, gain1_h, gain2_h, gain3_h, decay_h, wb_h, wi_h, ga_h, gx_h, wm_h,
    routes_h, rweight_h, eg_h, eu_h, ed_h, sg_h, su_h, sd_h,
    out_v, state_v, window_v,
    tok, lru, win, taps, gains, decay, wb, wi, gax, wm, routes, rweight,
    egu, ed, sgu, sd,
    middle_v, ffn,
    mix_s, mix_r, meta_s, meta_r, sh_s, sh_r,
    g_buf, r_buf, x_buf, p_buf, whi, wlo, hid_v, y_s, y_r, o_buf, b_buf, t_buf, rl_buf, c_buf, v_buf, rt_buf,
    lsem, core_s, chip_s, meta_sem, mix_r_sem, sh_r_sem, rt_r_sem,
    za_two, za_r, xa_r, xf_r, yx_r, xb_r, zb_two, zb_r,
):
    me = lax.axis_index("ep")
    c = lax.axis_index("tp")
    z = me // NQ
    q = me % NQ
    y, x = q // 4, q % 4

    def z_peer(i):
        return lax.rem(z + (i + NZ), NZ)

    y_peer = [lax.rem(y + i, 4) * 4 for i in range(4)]
    x_peer = [lax.rem(x + i, 4) for i in range(4)]

    def q_peer(i):
        return y_peer[i // 4] + x_peer[i % 4]

    def rows(i, n):
        return pl.ds(pl.multiple_of(i * n, n), n)

    count = iter(range(NLOAD))

    def load(*pairs):
        k = next(count)
        copies = [pltpu.make_async_copy(src, dst, lsem.at[k]) for src, dst in pairs]
        for copy in copies:
            copy.start()
        return k, copies[0]

    def loaded(group, whole=None):
        k, copy = group
        if whole is not None:
            copy = pltpu.make_async_copy(whole, whole, lsem.at[k])
        copy.wait()

    l_tok = load((tok_h, tok))
    l_gain0 = load((gain0_h, gains.at[0]))
    l_wi = [load((wi_h.at[pl.ds(i, n)], wi.at[pl.ds(i, n)])) for i, n in PIECES]
    l_win = load((win_h, win))
    l_taps = load((taps_h, taps))
    l_gax = load((ga_h, gax.at[0]), (gx_h, gax.at[1]))
    l_decay = load((decay_h, decay))
    l_lru = load((lru_h, lru))
    l_wb = load((wb_h, wb))
    l_wm = [load((wm_h.at[:, pl.ds(i * HALF, HALF)], wm.at[i])) for i in range(2)]
    l_routes = load((routes_h, routes))
    l_rweight = load((rweight_h, rweight))
    l_gains = load((gain1_h, gains.at[1]), (gain2_h, gains.at[2]), (gain3_h, gains.at[3]))

    barrier = pltpu.get_barrier_semaphore()
    pl.semaphore_signal(barrier, inc=1, device_id=(me, 1 - c), device_id_type=MESH)

    def greet_z(i, carry):
        pl.semaphore_signal(barrier, inc=1, device_id=(z_peer(i) * NQ + q, c), device_id_type=MESH)
        return carry

    lax.fori_loop(1, NZ, greet_z, 0)
    for i in FAR:
        pl.semaphore_signal(barrier, inc=1, device_id=(z * NQ + q_peer(i), c), device_id_type=MESH)

    loaded(l_tok)
    loaded(l_gain0)
    normed = scaled(tok[...].astype(F32), gains[0]).astype(BF16)
    inflow = jnp.zeros((SEQ, LC), F32)
    for group, (i, n) in zip(l_wi, PIECES):
        loaded(group)
        inflow += dot(normed[:, i : i + n], wi[i : i + n, :])
    inflow = inflow.astype(BF16)
    loaded(l_win)
    loaded(l_taps)
    conv = inflow.astype(F32) * taps[3:4, :].astype(F32)
    for j in range(3):
        conv += win[j].astype(F32) * taps[j : j + 1, :].astype(F32)
        window_v[j] = win[j + 1] if j < 2 else inflow
    low = conv.astype(BF16)
    loaded(l_gax, gax)
    loaded(l_decay)
    loaded(l_lru)
    loaded(l_wb)
    branch = dot(normed, wb[...])
    groups = LC // 128
    recur = [dot(low[:, g * 128 : (g + 1) * 128], gax[0, g]) for g in range(groups)]
    inputs = [dot(low[:, g * 128 : (g + 1) * 128], gax[1, g]) for g in range(groups)]
    recur_gate = jax.nn.sigmoid(jnp.concatenate(recur, axis=1))
    input_gate = jax.nn.sigmoid(jnp.concatenate(inputs, axis=1))
    fall = 8.0 * recur_gate * decay[...]
    t = jnp.tanh(fall)
    state = jnp.exp(-fall) * lru[...] + jnp.sqrt(2.0 * t / (1.0 + t)) * conv * input_gate
    state_v[...] = state
    gated = (state * jax.nn.gelu(branch)).astype(BF16)
    for i in range(2):
        loaded(l_wm[i])
        mix_s[i] = dot(gated, wm[i]).astype(BF16)

    l_sgu = load((sg_h, sgu.at[0]), (su_h, sgu.at[1]))
    l_sd = load((sd_h, sd))
    l_egu = load((eg_h.at[0], egu.at[0]), (eu_h.at[0], egu.at[1]))
    l_ed = load(*[(ed_h.at[:, pl.ds(i * HALF, HALF)], ed.at[i]) for i in range(2)])

    pl.semaphore_wait(barrier, 1 + (NZ - 1) + (NQ - 1))

    def remote(src, dst, ssem, rsem, e, t):
        return pltpu.make_async_remote_copy(
            src_ref=src, dst_ref=dst, send_sem=ssem, recv_sem=rsem, device_id=(e, t), device_id_type=MESH
        )

    def to_z(src, dst, rsem, i):
        return remote(src, dst, chip_s, rsem, z_peer(i) * NQ + q, c)

    def to_core(src, dst, rsem):
        return remote(src, dst, core_s, rsem, me, 1 - c)

    def arrived(ref, rsem):
        to_core(ref, ref, rsem).wait_recv()

    mix_copies = [to_core(mix_s.at[i], mix_r.at[i], mix_r_sem.at[i]) for i in range(2)]
    for copy in mix_copies:
        copy.start()

    with jax.named_scope("slots"):
        loaded(l_routes)
        loaded(l_rweight)
        lane = lax.broadcasted_iota(jnp.int32, (1, NZ * SEQ), 1)
        mine = (lane // SEQ) == z
        earlier = lax.broadcasted_iota(jnp.int32, (SEQ, NZ * SEQ), 0) < (lane % SEQ)
        diagonal = lax.broadcasted_iota(jnp.int32, (SEQ, SEQ), 0) == lax.broadcasted_iota(jnp.int32, (SEQ, SEQ), 1)
        narrow = routes[...].astype(F32)
        named = [
            jnp.sum(jnp.where(diagonal, narrow[k : k + 1, :], 0.0), axis=1, keepdims=True) for k in range(TOP)
        ]
        wide = jnp.concatenate([narrow] * NZ, axis=1)
        for k in range(TOP):
            expert = wide[k : k + 1, :]
            same = named[0] == expert
            for j in range(1, TOP):
                same = same | (named[j] == expert)
            rank = jnp.sum(jnp.where(same & earlier, 1.0, 0.0), axis=0, keepdims=True)
            meta_s[k : k + 1, :] = jnp.where(mine, 2.0 * expert + rank, 0.0)
        meta_s[TOP : 2 * TOP, :] = jnp.where(mine, jnp.concatenate([rweight[...]] * NZ, axis=1), 0.0)
        meta_r[pl.ds(z, 1)] = meta_s[...][None]

    def meta_send(i, carry):
        remote(meta_s, meta_r.at[z], meta_sem.at[0], meta_sem.at[1], z_peer(i) * NQ + q, c).start()
        return carry

    lax.fori_loop(1, NZ, meta_send, 0)

    loaded(l_gains, gains.at[pl.ds(1, 3)])
    mixed = []
    for i in range(2):
        mix_copies[i].wait_recv()
        mixed.append(mix_s[i].astype(F32) + mix_r[i].astype(F32))
    mixed = jnp.concatenate(mixed, axis=1)
    middle = (tok[...].astype(F32) + scaled(mixed, gains[1])).astype(BF16)
    middle_v[...] = middle
    ffn[...] = scaled(middle.astype(F32), gains[2]).astype(BF16)

    def z_copy(ch, source, i, rsem):
        block = g_buf[ch].at[rows(source, SEQ)]
        return to_z(block, block, rsem, i)

    def direct(ch):
        columns = pl.ds(pl.multiple_of(c * HALF + STARTS[ch], 128), WIDTHS[ch])
        g_buf[ch][rows(z, SEQ), :] = ffn[:, columns]
        z_copy(ch, z, 2, za_two.at[ch]).start()
        z_copy(ch, z, -2, za_two.at[ch]).start()
        z_copy(ch, z, 1, za_r.at[ch]).start()
        z_copy(ch, z, -1, za_r.at[ch]).start()

    def relay(ch):
        arrived(g_buf[ch].at[pl.ds(0, 2 * SEQ)], za_two.at[ch])
        for way in range(2):
            sign = 1 - 2 * way
            source = z_peer(-2 * sign)
            if PLUS[ch] == way:
                z_copy(ch, source, 2 * sign, za_r.at[ch]).start()
            z_copy(ch, source, sign, za_r.at[ch]).start()

    for ch in range(NCH - 1):
        direct(ch)

    loaded(l_sgu, sgu)
    loaded(l_sd)
    hidden = (jax.nn.silu(dot(ffn[...], sgu[0])) * dot(ffn[...], sgu[1])).astype(BF16)
    sh_s[...] = dot(hidden, sd[...]).astype(BF16)
    to_core(sh_s, sh_r, sh_r_sem).start()

    relay(0)
    direct(NCH - 1)
    relay(1)

    many = meta_r.at[pl.ds(0, NZ - 1)]
    remote(many, many, meta_sem.at[0], meta_sem.at[1], z_peer(1) * NQ + q, c).wait()
    meta = jnp.sum(meta_r[...], axis=0)
    code = meta[0:TOP, :].astype(jnp.int32)
    place = ((code % (2 * NQ)) // 2) * ROWS + (lane // SEQ) * 2 + code % 2
    place = jnp.where(code // (2 * NQ) == z, place, -1)
    row = lax.broadcasted_iota(jnp.int32, (NQ * ROWS, NZ * SEQ), 0)
    filled = jnp.zeros((NQ * ROWS, NZ * SEQ), F32)
    weight = jnp.zeros((NQ * ROWS, NZ * SEQ), F32)
    for k in range(TOP):
        hit = row == place[k : k + 1, :]
        filled = jnp.where(hit, 1.0, filled)
        weight = jnp.where(hit, meta[TOP + k : TOP + k + 1, :], weight)
    p_buf[...] = filled.astype(BF16)
    weight = weight.T
    high = weight.astype(BF16)
    whi[...] = high
    wlo[...] = (weight - high.astype(F32)).astype(BF16)

    def q_send(src, dst, rsem):
        for i in FAR:
            p = q_peer(i)
            remote(src.at[rows(p, ROWS)], dst.at[rows(q, ROWS)], chip_s, rsem, z * NQ + p, c).start()

    others = pl.ds(0, (NQ - 1) * ROWS)

    def picked(ch):
        arrived(g_buf[ch].at[pl.ds(0, 5 * SEQ)], za_r.at[ch])
        r_buf[ch][...] = dot(p_buf[...], g_buf[ch][...]).astype(BF16)
        q_send(r_buf[ch], x_buf[ch].at[c], xa_r.at[ch])
        x_buf[ch][c, rows(q, ROWS), :] = r_buf[ch][rows(q, ROWS), :]

    for ch in range(2, NCH):
        relay(ch)
        picked(ch - 2)
    picked(NCH - 2)
    picked(NCH - 1)

    loaded(l_egu, egu)
    gate = jnp.zeros((NQ * ROWS, HID), F32)
    up = jnp.zeros((NQ * ROWS, HID), F32)
    early = pl.ds(0, STARTS[-1])
    for ch in range(NCH):
        arrived(x_buf[ch].at[c, others], xa_r.at[ch])
        to_core(x_buf[ch].at[c], x_buf[ch].at[c], xf_r.at[ch // (NCH - 1)]).start()
        depth = pl.ds(pl.multiple_of(c * HALF + STARTS[ch], 128), WIDTHS[ch])
        gate += dot(x_buf[ch][c], egu[0, depth, :])
        up += dot(x_buf[ch][c], egu[1, depth, :])
    for ch in range(NCH):
        if ch == 0:
            arrived(wm.at[0, pl.ds(0, NQ * ROWS), early], xf_r.at[0])
        if ch == NCH - 1:
            arrived(x_buf[ch].at[1 - c], xf_r.at[1])
        depth = pl.ds(pl.multiple_of((1 - c) * HALF + STARTS[ch], 128), WIDTHS[ch])
        gate += dot(x_buf[ch][1 - c], egu[0, depth, :])
        up += dot(x_buf[ch][1 - c], egu[1, depth, :])
    hid_v[...] = (jax.nn.silu(gate) * up).astype(BF16)

    loaded(l_ed, ed)

    def down(core, ch):
        return dot(hid_v[...], ed[core, :, STARTS[ch] : STARTS[ch] + WIDTHS[ch]]).astype(BF16)

    def trade(ch):
        y_s[ch][...] = down(1 - c, ch)
        to_core(y_s[ch], y_r[ch], yx_r.at[ch]).start()

    def back(ch):
        own = down(c, ch).astype(F32)
        arrived(y_r[ch], yx_r.at[ch])
        o_buf[ch][...] = (own + y_r[ch][...].astype(F32)).astype(BF16)
        q_send(o_buf[ch], b_buf[ch], xb_r.at[ch])
        b_buf[ch][rows(q, ROWS), :] = o_buf[ch][rows(q, ROWS), :]

    trade(0)
    for ch in range(1, NCH):
        trade(ch)
        back(ch - 1)
    back(NCH - 1)

    def weighted(ch):
        arrived(b_buf[ch].at[others], xb_r.at[ch])
        t_buf[ch][...] = (dot(whi[...], b_buf[ch][...]) + dot(wlo[...], b_buf[ch][...])).astype(BF16)
        if ch == NCH - 1:
            for slot, i in enumerate((4, 3, -3, 2, -2, 1, -1)):
                to_z(t_buf[ch].at[rows(z_peer(i), SEQ)], v_buf[ch].at[slot], zb_r.at[1], i).start()
            return
        for way in range(2):
            sign = 1 - 2 * way
            if PLUS[ch] == way:
                to_z(t_buf[ch].at[rows(z_peer(4), SEQ)], rl_buf[ch].at[2], zb_two.at[ch], -2 * sign).start()
            to_z(t_buf[ch].at[rows(z_peer(-3 * sign), SEQ)], rl_buf[ch].at[way], zb_two.at[ch], -sign).start()
        for way in range(2):
            sign = 1 - 2 * way
            to_z(t_buf[ch].at[rows(z_peer(-sign), SEQ)], v_buf[ch].at[way], zb_r.at[0], -sign).start()

    def relayed(ch):
        arrived(rl_buf[ch], zb_two.at[ch])
        for way in range(2):
            sign = 1 - 2 * way
            total = t_buf[ch][rows(z_peer(-2 * sign), SEQ), :].astype(F32) + rl_buf[ch][way].astype(F32)
            if PLUS[ch] == way:
                total += rl_buf[ch][2].astype(F32)
            c_buf[ch][way] = total.astype(BF16)
            to_z(c_buf[ch].at[way], v_buf[ch].at[2 + way], zb_r.at[0], -2 * sign).start()

    weighted(0)
    for ch in range(1, NCH):
        weighted(ch)
        relayed(ch - 1)

    arrived(sh_r, sh_r_sem)

    def half(h):
        return pl.ds(pl.multiple_of(h * HALF, HALF), HALF)

    for ch in range(NCH):
        if ch == 0:
            arrived(wm.at[0, pl.ds(0, 4 * SEQ), early], zb_r.at[0])
        if ch == NCH - 1:
            arrived(v_buf[ch], zb_r.at[1])
        total = t_buf[ch][rows(z, SEQ), :].astype(F32)
        for s in range(7 if ch == NCH - 1 else 4):
            total += v_buf[ch][s].astype(F32)
        rt_buf[ch][c] = total.astype(BF16)
        to_core(rt_buf[ch].at[c], rt_buf[ch].at[c], rt_r_sem).start()

    def routed_and_shared(h):
        routed = jnp.concatenate([rt_buf[ch][h] for ch in range(NCH)], axis=1).astype(F32)
        return routed + (sh_s[:, half(h)].astype(F32) + sh_r[:, half(h)].astype(F32))

    def squares(value):
        return jnp.sum(value * value, axis=-1, keepdims=True)

    own = routed_and_shared(c)
    own_squares = squares(own)

    part = wm.at[:, pl.ds(0, (7 * SEQ + (NQ - 1) * ROWS))]
    to_z(part, part, zb_r.at[0], 1).wait_send()

    arrived(wm.at[0, pl.ds(0, SEQ)], rt_r_sem)
    other = routed_and_shared(1 - c)
    scale = lax.rsqrt((own_squares + squares(other)) / D + 1e-06)
    for h, value in ((c, own), (1 - c, other)):
        last = value * scale * gains[3, :, half(h)]
        out_v[:, half(h)] = (middle_v[:, half(h)].astype(F32) + last).astype(BF16)
    part = wm.at[:, pl.ds(0, (5 * SEQ + 2 * NQ * ROWS) // 2)]
    to_core(part, part, rt_r_sem).wait_send()


def store(*refs):
    n = len(refs) // 2
    copies = [pltpu.make_async_copy(refs[i], refs[n + i], refs[-1].at[i]) for i in range(n)]
    for copy in copies:
        copy.start()
    for copy in copies:
        copy.wait()


def on_device(
    tokens, lru_state, conv_window, gain_mix_in, gain_mix_out, gain_ffn_in, gain_ffn_out, w_branch, w_input,
    conv_taps, gate_a, gate_x, decay_rate, w_mix_out, routes, route_weight, expert_gate, expert_up, expert_down,
    shared_gate, shared_up, shared_down,
):
    hbm = pl.BlockSpec(memory_space=pltpu.HBM)

    def vmem(*shape, dtype=BF16):
        return pltpu.VMEM(shape, dtype)

    def chunks(*shape):
        return [vmem(*shape, width) for width in WIDTHS]

    def dma(*shape):
        return pltpu.SemaphoreType.DMA(shape)

    one = pltpu.SemaphoreType.DMA
    scratch = [
        vmem(SEQ, D), vmem(SEQ, LC, dtype=F32), vmem(3, SEQ, LC), vmem(4, LC), vmem(4, 1, D, dtype=F32),
        vmem(1, LC, dtype=F32), vmem(D, LC), vmem(D, LC), vmem(2, 4, 128, 128), vmem(2, LC, HALF),
        vmem(TOP, SEQ, dtype=jnp.int32), vmem(TOP, SEQ, dtype=F32),
        vmem(2, D, HID), vmem(2, HID, HALF), vmem(2, D, HID), vmem(HID, D),
        vmem(SEQ, D), vmem(SEQ, D),
        vmem(2, SEQ, HALF), vmem(2, SEQ, HALF), vmem(2 * TOP, NZ * SEQ, dtype=F32), vmem(NZ, 2 * TOP, NZ * SEQ, dtype=F32),
        vmem(SEQ, D), vmem(SEQ, D),
        chunks(NZ * SEQ), chunks(NQ * ROWS), chunks(2, NQ * ROWS),
        vmem(NQ * ROWS, NZ * SEQ), vmem(NZ * SEQ, NQ * ROWS), vmem(NZ * SEQ, NQ * ROWS), vmem(NQ * ROWS, HID),
        chunks(NQ * ROWS), chunks(NQ * ROWS), chunks(NQ * ROWS), chunks(NQ * ROWS),
        chunks(NZ * SEQ), chunks(3, SEQ), chunks(2, SEQ),
        [vmem(7 if ch == NCH - 1 else 4, SEQ, WIDTHS[ch]) for ch in range(NCH)], chunks(2, SEQ),
        dma(NLOAD), one, one, dma(2), dma(2), one, one,
        dma(NCH), dma(NCH), dma(NCH), dma(2), dma(NCH), dma(NCH), dma(NCH - 1), dma(2),
    ]
    vm = pl.BlockSpec(memory_space=pltpu.VMEM)
    results = pl.pallas_call(
        kernel,
        out_shape=(
            pltpu.VMEM((SEQ, D), BF16),
            pltpu.VMEM((SEQ, LC), F32),
            pltpu.VMEM((3, SEQ, LC), BF16),
        ),
        in_specs=[hbm] * 22,
        out_specs=(vm,) * 3,
        scratch_shapes=scratch,
        compiler_params=pltpu.CompilerParams(collective_id=0, has_side_effects=True, vmem_limit_bytes=60 * 2**20),
        name="layer",
    )(
        tokens, lru_state, conv_window.transpose(1, 0, 2), conv_taps, gain_mix_in[None], gain_mix_out[None],
        gain_ffn_in[None], gain_ffn_out[None], decay_rate[None], w_branch, w_input, gate_a, gate_x, w_mix_out,
        routes.T, route_weight.T, expert_gate, expert_up, expert_down[0], shared_gate, shared_up, shared_down,
    )
    layer_out, new_state, window = pl.pallas_call(
        store,
        out_shape=tuple(jax.ShapeDtypeStruct(r.shape, r.dtype) for r in results),
        in_specs=[vm] * 3,
        out_specs=(hbm,) * 3,
        scratch_shapes=[dma(3)],
        compiler_params=pltpu.CompilerParams(has_side_effects=True, vmem_limit_bytes=2**20),
        name="store",
    )(*results)
    return (layer_out, new_state, window.transpose(1, 0, 2))


def solution(mesh):
    placed = (
        P("ep", None),
        P("ep", "tp"),
        P("ep", None, "tp"),
        P(),
        P(),
        P(),
        P(),
        P(None, "tp"),
        P(None, "tp"),
        P(None, "tp"),
        P("tp", None, None),
        P("tp", None, None),
        P("tp"),
        P("tp", None),
        P("ep", None),
        P("ep", None),
        P("ep", None, "tp"),
        P("ep", None, "tp"),
        P("ep", "tp", None),
        P(None, "tp"),
        P(None, "tp"),
        P("tp", None),
    )
    return jax.shard_map(
        on_device,
        mesh=mesh,
        in_specs=placed,
        out_specs=(P("ep", None), P("ep", "tp"), P("ep", None, "tp")),
        check_vma=False,
    )
```

time: 53.9 us -> 52.5 us (0.974)
  Pallas kernels: 53.2 us -> 51.8 us
    pallas_call x1, Pallas kernels: 52.4 us -> 51.1 us  [on_device(): pl.pallas_call(kernel, out_shape=(pltpu.VMEM((SEQ, D), BF16), pltpu.VMEM(...]
where the time goes in v5:
time: 52.5 us; the launch traced here: 52.4 us
  Pallas kernels  51.8 us (99%)
  between operations  0.65 us (1%)
    pallas_call x1, Pallas kernels, on_device(): pl.pallas_call(kernel, out_shape=(pltpu.VMEM((SEQ, D), BF16), pltpu.VMEM(...  51.1 us

profile of v5, /device:TPU:1, one launch (start us, length us, event | category | flops | bytes accessed | tf_op | source)
XLA Modules:
  0.0 52.4 jit_solution(4427378550108801198)
XLA Ops:
  0.6 51.1 %layer.1 = (bf16[32,2048]{1,0:T(8,128)(2,1)S(1)}, f32[32,512]{1,0:T(8,128)S(1)}, bf16[3,32,512]{2,1,0:T(8,128)(2,1)S(1)}) custom-call(bf16[32,2048]{1,0:T(8,128)(2,1)} %tok_h.1, f32[32,512]{1,0:T(8,128)} %lru_h.1, bf16[3,32,512]{2,1,0:T(8,128)(2,1)} %bitcast.11, bf16[4,512]{1,0:T(4,128)(2,1)} %taps_h.1, f32[1,2048]{1,0:T(1,128)} %bitcast.12, ...), custom_call_target="tpu_custom_call" | custom-call | tf_op jit(solution)/shard_map/layer/pallas_call | solution.py:434
  51.7 0.7 %store.1 = (bf16[32,2048]{1,0:T(8,128)(2,1)}, f32[32,512]{1,0:T(8,128)}, bf16[3,32,512]{2,1,0:T(8,128)(2,1)}) custom-call(bf16[32,2048]{1,0:T(8,128)(2,1)S(1)} %get-tuple-element.9.refs_0_, f32[32,512]{1,0:T(8,128)S(1)} %get-tuple-element.10.refs_1_, bf16[3,32,512]{2,1,0:T(8,128)(2,1)S(1)} %get-tuple-element.11.refs_2_), custom_call_target="tpu_custom_call" | custom-call | tf_op jit(solution)/shard_map/store/pallas_call | solution.py:451

commit v6 on v5

--- a/solution.py
+++ b/solution.py
@@ -17,16 +17,18 @@
 TOP = 4
 D = 2048
 HALF = D // 2
-WIDTHS = (256, 512, 256)
+WIDTHS = (256, 256, 256, 256)
 NCH = len(WIDTHS)
 STARTS = tuple(sum(WIDTHS[:i]) for i in range(NCH))
+BACK_WIDTHS = (256, 512, 256)
+NB = len(BACK_WIDTHS)
+BACK_STARTS = tuple(sum(BACK_WIDTHS[:i]) for i in range(NB))
 FAR = (10, 11, 9, 14, 6, 15, 5, 13, 7, 2, 8, 3, 1, 12, 4)
 LC = 512
 HID = 256
 ROWS = NZ * 2
-NLOAD = 20
-PLUS = (0, 1, 0)
-PIECES = ((0, 768), (768, 768), (1536, 512))
+NLOAD = 24
+PIECES = ((0, 512), (512, 512), (1024, 512), (1536, 512))
 
 
 def scaled(value, gain):
@@ -90,7 +92,7 @@
     l_gax = load((ga_h, gax.at[0]), (gx_h, gax.at[1]))
     l_decay = load((decay_h, decay))
     l_lru = load((lru_h, lru))
-    l_wb = load((wb_h, wb))
+    l_wb = [load((wb_h.at[pl.ds(i, n)], wb.at[pl.ds(i, n)])) for i, n in PIECES]
     l_wm = [load((wm_h.at[:, pl.ds(i * HALF, HALF)], wm.at[i])) for i in range(2)]
     l_routes = load((routes_h, routes))
     l_rweight = load((rweight_h, rweight))
@@ -125,8 +127,6 @@
     loaded(l_gax, gax)
     loaded(l_decay)
     loaded(l_lru)
-    loaded(l_wb)
-    branch = dot(normed, wb[...])
     groups = LC // 128
     recur = [dot(low[:, g * 128 : (g + 1) * 128], gax[0, g]) for g in range(groups)]
     inputs = [dot(low[:, g * 128 : (g + 1) * 128], gax[1, g]) for g in range(groups)]
@@ -136,6 +136,10 @@
     t = jnp.tanh(fall)
     state = jnp.exp(-fall) * lru[...] + jnp.sqrt(2.0 * t / (1.0 + t)) * conv * input_gate
     state_v[...] = state
+    branch = jnp.zeros((SEQ, LC), F32)
+    for group, (i, n) in zip(l_wb, PIECES):
+        loaded(group)
+        branch += dot(normed[:, i : i + n], wb[i : i + n, :])
     gated = (state * jax.nn.gelu(branch)).astype(BF16)
     for i in range(2):
         loaded(l_wm[i])
@@ -208,6 +212,9 @@
         block = g_buf[ch].at[rows(source, SEQ)]
         return to_z(block, block, rsem, i)
 
+    def side(width, way):
+        return pl.ds(way * width // 2, width // 2)
+
     def direct(ch):
         columns = pl.ds(pl.multiple_of(c * HALF + STARTS[ch], 128), WIDTHS[ch])
         g_buf[ch][rows(z, SEQ), :] = ffn[:, columns]
@@ -221,8 +228,8 @@
         for way in range(2):
             sign = 1 - 2 * way
             source = z_peer(-2 * sign)
-            if PLUS[ch] == way:
-                z_copy(ch, source, 2 * sign, za_r.at[ch]).start()
+            part = g_buf[ch].at[rows(source, SEQ), side(WIDTHS[ch], way)]
+            to_z(part, part, za_r.at[ch], 2 * sign).start()
             z_copy(ch, source, sign, za_r.at[ch]).start()
 
     for ch in range(NCH - 1):
@@ -299,7 +306,7 @@
     loaded(l_ed, ed)
 
     def down(core, ch):
-        return dot(hid_v[...], ed[core, :, STARTS[ch] : STARTS[ch] + WIDTHS[ch]]).astype(BF16)
+        return dot(hid_v[...], ed[core, :, BACK_STARTS[ch] : BACK_STARTS[ch] + BACK_WIDTHS[ch]]).astype(BF16)
 
     def trade(ch):
         y_s[ch][...] = down(1 - c, ch)
@@ -313,22 +320,22 @@
         b_buf[ch][rows(q, ROWS), :] = o_buf[ch][rows(q, ROWS), :]
 
     trade(0)
-    for ch in range(1, NCH):
+    for ch in range(1, NB):
         trade(ch)
         back(ch - 1)
-    back(NCH - 1)
+    back(NB - 1)
 
     def weighted(ch):
         arrived(b_buf[ch].at[others], xb_r.at[ch])
         t_buf[ch][...] = (dot(whi[...], b_buf[ch][...]) + dot(wlo[...], b_buf[ch][...])).astype(BF16)
-        if ch == NCH - 1:
+        if ch == NB - 1:
             for slot, i in enumerate((4, 3, -3, 2, -2, 1, -1)):
                 to_z(t_buf[ch].at[rows(z_peer(i), SEQ)], v_buf[ch].at[slot], zb_r.at[1], i).start()
             return
         for way in range(2):
             sign = 1 - 2 * way
-            if PLUS[ch] == way:
-                to_z(t_buf[ch].at[rows(z_peer(4), SEQ)], rl_buf[ch].at[2], zb_two.at[ch], -2 * sign).start()
+            part = side(BACK_WIDTHS[ch], way)
+            to_z(t_buf[ch].at[rows(z_peer(4), SEQ), part], rl_buf[ch].at[2, :, part], zb_two.at[ch], -2 * sign).start()
             to_z(t_buf[ch].at[rows(z_peer(-3 * sign), SEQ)], rl_buf[ch].at[way], zb_two.at[ch], -sign).start()
         for way in range(2):
             sign = 1 - 2 * way
@@ -339,13 +346,15 @@
         for way in range(2):
             sign = 1 - 2 * way
             total = t_buf[ch][rows(z_peer(-2 * sign), SEQ), :].astype(F32) + rl_buf[ch][way].astype(F32)
-            if PLUS[ch] == way:
-                total += rl_buf[ch][2].astype(F32)
-            c_buf[ch][way] = total.astype(BF16)
+            mid = BACK_WIDTHS[ch] // 2
+            far = rl_buf[ch][2, :, way * mid : (way + 1) * mid].astype(F32)
+            sides = [total[:, :mid], total[:, mid:]]
+            sides[way] += far
+            c_buf[ch][way] = jnp.concatenate(sides, axis=1).astype(BF16)
             to_z(c_buf[ch].at[way], v_buf[ch].at[2 + way], zb_r.at[0], -2 * sign).start()
 
     weighted(0)
-    for ch in range(1, NCH):
+    for ch in range(1, NB):
         weighted(ch)
         relayed(ch - 1)
 
@@ -354,19 +363,19 @@
     def half(h):
         return pl.ds(pl.multiple_of(h * HALF, HALF), HALF)
 
-    for ch in range(NCH):
+    for ch in range(NB):
         if ch == 0:
-            arrived(wm.at[0, pl.ds(0, 4 * SEQ), early], zb_r.at[0])
-        if ch == NCH - 1:
+            arrived(wm.at[0, pl.ds(0, 4 * SEQ), pl.ds(0, BACK_STARTS[-1])], zb_r.at[0])
+        if ch == NB - 1:
             arrived(v_buf[ch], zb_r.at[1])
         total = t_buf[ch][rows(z, SEQ), :].astype(F32)
-        for s in range(7 if ch == NCH - 1 else 4):
+        for s in range(7 if ch == NB - 1 else 4):
             total += v_buf[ch][s].astype(F32)
         rt_buf[ch][c] = total.astype(BF16)
         to_core(rt_buf[ch].at[c], rt_buf[ch].at[c], rt_r_sem).start()
 
     def routed_and_shared(h):
-        routed = jnp.concatenate([rt_buf[ch][h] for ch in range(NCH)], axis=1).astype(F32)
+        routed = jnp.concatenate([rt_buf[ch][h] for ch in range(NB)], axis=1).astype(F32)
         return routed + (sh_s[:, half(h)].astype(F32) + sh_r[:, half(h)].astype(F32))
 
     def squares(value):
@@ -407,8 +416,10 @@
     def vmem(*shape, dtype=BF16):
         return pltpu.VMEM(shape, dtype)
 
-    def chunks(*shape):
-        return [vmem(*shape, width) for width in WIDTHS]
+    def chunks(*shape, widths=WIDTHS):
+        return [vmem(*shape, width) for width in widths]
+
+    backs = functools.partial(chunks, widths=BACK_WIDTHS)
 
     def dma(*shape):
         return pltpu.SemaphoreType.DMA(shape)
@@ -424,11 +435,11 @@
         vmem(SEQ, D), vmem(SEQ, D),
         chunks(NZ * SEQ), chunks(NQ * ROWS), chunks(2, NQ * ROWS),
         vmem(NQ * ROWS, NZ * SEQ), vmem(NZ * SEQ, NQ * ROWS), vmem(NZ * SEQ, NQ * ROWS), vmem(NQ * ROWS, HID),
-        chunks(NQ * ROWS), chunks(NQ * ROWS), chunks(NQ * ROWS), chunks(NQ * ROWS),
-        chunks(NZ * SEQ), chunks(3, SEQ), chunks(2, SEQ),
-        [vmem(7 if ch == NCH - 1 else 4, SEQ, WIDTHS[ch]) for ch in range(NCH)], chunks(2, SEQ),
+        backs(NQ * ROWS), backs(NQ * ROWS), backs(NQ * ROWS), backs(NQ * ROWS),
+        backs(NZ * SEQ), backs(3, SEQ), backs(2, SEQ),
+        [vmem(7 if ch == NB - 1 else 4, SEQ, BACK_WIDTHS[ch]) for ch in range(NB)], backs(2, SEQ),
         dma(NLOAD), one, one, dma(2), dma(2), one, one,
-        dma(NCH), dma(NCH), dma(NCH), dma(2), dma(NCH), dma(NCH), dma(NCH - 1), dma(2),
+        dma(NCH), dma(NCH), dma(NCH), dma(2), dma(NB), dma(NB), dma(NB - 1), dma(2),
     ]
     vm = pl.BlockSpec(memory_space=pltpu.VMEM)
     results = pl.pallas_call(

time: 52.5 us -> 51.4 us (0.979)
  Pallas kernels: 51.8 us -> 50.7 us
    pallas_call x1, Pallas kernels: 51.1 us -> 49.9 us  [on_device(): pl.pallas_call(kernel, out_shape=(pltpu.VMEM((SEQ, D), BF16), pltpu.VMEM(...]
where the time goes in v6:
time: 51.4 us; the launch traced here: 51.3 us
  Pallas kernels  50.7 us (99%)
  between operations  0.65 us (1%)
    pallas_call x1, Pallas kernels, on_device(): pl.pallas_call(kernel, out_shape=(pltpu.VMEM((SEQ, D), BF16), pltpu.VMEM(...  49.9 us

profile of v6, /device:TPU:1, one launch (start us, length us, event | category | flops | bytes accessed | tf_op | source)
XLA Modules:
  0.0 51.3 jit_solution(7257497546484596066)
XLA Ops:
  0.6 49.9 %layer.1 = (bf16[32,2048]{1,0:T(8,128)(2,1)S(1)}, f32[32,512]{1,0:T(8,128)S(1)}, bf16[3,32,512]{2,1,0:T(8,128)(2,1)S(1)}) custom-call(bf16[32,2048]{1,0:T(8,128)(2,1)} %tok_h.1, f32[32,512]{1,0:T(8,128)} %lru_h.1, bf16[3,32,512]{2,1,0:T(8,128)(2,1)} %bitcast.11, bf16[4,512]{1,0:T(4,128)(2,1)} %taps_h.1, f32[1,2048]{1,0:T(1,128)} %bitcast.12, ...), custom_call_target="tpu_custom_call" | custom-call | tf_op jit(solution)/shard_map/layer/pallas_call | solution.py:445
  50.6 0.7 %store.1 = (bf16[32,2048]{1,0:T(8,128)(2,1)}, f32[32,512]{1,0:T(8,128)}, bf16[3,32,512]{2,1,0:T(8,128)(2,1)}) custom-call(bf16[32,2048]{1,0:T(8,128)(2,1)S(1)} %get-tuple-element.9.refs_0_, f32[32,512]{1,0:T(8,128)S(1)} %get-tuple-element.10.refs_1_, bf16[3,32,512]{2,1,0:T(8,128)(2,1)S(1)} %get-tuple-element.11.refs_2_), custom_call_target="tpu_custom_call" | custom-call | tf_op jit(solution)/shard_map/store/pallas_call | solution.py:462
